TPU v7x, 256 devices: a whole 4x4x8 slice. The times are simulated.
256 devices in a mesh: ep: 64 (over z, y, core), tp: 4 (over x).
Axes of the slice: x: 4, y: 4, z: 8, core: 2. Of those that a mesh axis runs over, the one named last changes fastest.
Arguments:
- tokens: bfloat16 [512, 1024], P('ep'), may hold values from -6 to 6
- ssm_state: float32 [512, 32, 64, 128], P('ep', 'tp'), may hold values from -6 to 6
- conv_x: bfloat16 [512, 3, 2048], P('ep', None, 'tp'), may hold values from -6 to 6
- conv_b: bfloat16 [512, 3, 1024], P('ep', None, 'tp'), may hold values from -6 to 6
- conv_c: bfloat16 [512, 3, 1024], P('ep', None, 'tp'), may hold values from -6 to 6
- w_x: bfloat16 [1024, 2048], P(None, 'tp'), may hold values from -0.1875 to 0.1875
- w_z: bfloat16 [1024, 2048], P(None, 'tp'), may hold values from -0.1875 to 0.1875
- w_b: bfloat16 [1024, 1024], P(None, 'tp'), may hold values from -0.1875 to 0.1875
- w_c: bfloat16 [1024, 1024], P(None, 'tp'), may hold values from -0.1875 to 0.1875
- w_dt: bfloat16 [1024, 32], replicated, may hold values from -0.1875 to 0.1875
- dt_bias: float32 [32], P('tp'), may hold values from -2 to 1
- a_log: float32 [32], P('tp'), may hold values from -3 to 1
- d_skip: float32 [32], P('tp'), may hold values from 0.1 to 1.9
- taps_x: bfloat16 [4, 2048], P(None, 'tp'), may hold values from -3 to 3
- taps_b: bfloat16 [4, 1024], P(None, 'tp'), may hold values from -3 to 3
- taps_c: bfloat16 [4, 1024], P(None, 'tp'), may hold values from -3 to 3
- norm1_gain: float32 [1024], replicated, may hold values from 0.1 to 1.9
- group_gain: float32 [2048], P('tp'), may hold values from 0.1 to 1.9
- w_out: bfloat16 [2048, 1024], P('tp'), may hold values from -0.125 to 0.125
- norm2_gain: float32 [1024], replicated, may hold values from 0.1 to 1.9
- route_ids: int32 [512, 6], P('ep'), may hold values from 0 to 63, all different within a row; in each aligned block of 8 rows (0 to 7, 8 to 15, ...) at most 2 rows name the same one
- route_weights: float32 [512, 6], P('ep'), may hold values from 0.1 to 1
- exp_gate: bfloat16 [64, 1024, 512], P('ep', None, 'tp'), may hold values from -0.1875 to 0.1875
- exp_up: bfloat16 [64, 1024, 512], P('ep', None, 'tp'), may hold values from -0.1875 to 0.1875
- exp_down: bfloat16 [64, 512, 1024], P('ep', 'tp'), may hold values from -0.25 to 0.25
- dense_gate: bfloat16 [1024, 1024], P('ep', 'tp'), may hold values from -0.1875 to 0.1875
- dense_up: bfloat16 [1024, 1024], P('ep', 'tp'), may hold values from -0.1875 to 0.1875
- dense_down: bfloat16 [1024, 1024], P('tp', 'ep'), may hold values from -0.1875 to 0.1875
- branch_gate: bfloat16 [1024], replicated, may hold values from -0.375 to 0.375
Outputs:
- mixed: bfloat16 [512, 1024], P('ep', 'tp')
- state_next: float32 [512, 32, 64, 128], P('ep', 'tp')
- conv_x_next: bfloat16 [512, 3, 2048], P('ep', None, 'tp')
- conv_b_next: bfloat16 [512, 3, 1024], P('ep', None, 'tp')
- conv_c_next: bfloat16 [512, 3, 1024], P('ep', None, 'tp')
Inputs may be any that keep to these rules, and one draw needn't show every extreme that they name: `route_ids`: each row names 6 different experts. Among the rows of one device no expert is named by more than 2 rows, a bound that some block reaches.
All inputs are finite; a program needn't handle non-finite values.
Results may differ from a plain program's by a relative error of at most 0.019.
Values may be sent and summed in bfloat16 or wider, within the bound.
A program may use at most 64 MiB of HBM per device.

v0:
```python
import jax
import jax.numpy as jnp
from jax import lax
from jax.sharding import Mesh
from jax.sharding import PartitionSpec as P

EP = ("ep_0", "ep_1", "ep_2")


epsilon = 1e-06


def copy_for_each(shard, axis):
    size = lax.axis_size(axis)
    return lax.all_to_all(
        jnp.broadcast_to(shard[None], (size, *shard.shape)), axis, 0, 0, tiled=True
    )


def over_copies(shard, axis):
    return copy_for_each(shard, axis).astype(jnp.float32).sum(axis=0)


def cut_along(shard, dim, size):
    before, after = (shard.shape[:dim], shard.shape[dim + 1 :])
    return jnp.moveaxis(shard.reshape(*before, size, -1, *after), dim, 0)


def sum_at_owner(shard, axis, dim):
    pieces = cut_along(shard, dim, lax.axis_size(axis))
    arrived = lax.all_to_all(pieces, axis, split_axis=0, concat_axis=0, tiled=True)
    return arrived.astype(jnp.float32).sum(axis=0)


def sent_together(arrays, axis, dim, along):
    ends, at = ([], 0)
    for a in arrays[:-1]:
        at += a.shape[along]
        ends.append(at)
    both = jnp.concatenate(arrays, axis=along)
    return tuple(jnp.split(lax.all_gather(both, axis, axis=dim, tiled=True), ends, axis=along))


def joined_along(pieces, dim):
    pieces = jnp.moveaxis(pieces, 0, dim)
    dims = pieces.shape
    return pieces.reshape(*dims[:dim], dims[dim] * dims[dim + 1], *dims[dim + 2 :])


def all_blocks(shard, axes, sequence):
    pieces = shard[None]
    for k in sequence:
        pieces = lax.all_gather(pieces, axes[k], axis=0, tiled=True)
    block = [lax.axis_size(axes[k]) for k in reversed(sequence)]
    pieces = pieces.reshape(*block, *shard.shape)
    turned = sorted(range(len(sequence)), key=lambda place: sequence[len(sequence) - 1 - place])
    return pieces.transpose(*turned, *range(len(sequence), pieces.ndim)).reshape(-1, *shard.shape)


def gather_axes(shard, axes, sequence, dim):
    return joined_along(all_blocks(shard, axes, sequence), dim)


def rms_rows(values, gain):
    return values * lax.rsqrt(jnp.mean(values * values, axis=-1, keepdims=True) + epsilon) * gain


def short_conv(previous, fresh, taps):
    window = jnp.concatenate((previous, fresh[:, None]), axis=1)
    summed = jnp.sum(window.astype(jnp.float32) * taps.astype(jnp.float32)[None], axis=1)
    return (jax.nn.silu(summed), window[:, 1:])


def mixer_core(
    x_new,
    z_new,
    b_new,
    c_new,
    dt_raw,
    ssm_state,
    conv_x,
    conv_b,
    conv_c,
    dt_bias,
    a_log,
    d_skip,
    taps_x,
    taps_b,
    taps_c,
    group_gain,
):
    seqs, heads, head_dim, state_dim = ssm_state.shape
    groups = b_new.shape[1] // state_dim
    x_conv, conv_x_next = short_conv(conv_x, x_new, taps_x)
    b_conv, conv_b_next = short_conv(conv_b, b_new, taps_b)
    c_conv, conv_c_next = short_conv(conv_c, c_new, taps_c)
    x_heads = x_conv.reshape(seqs, heads, head_dim)
    b_heads = jnp.repeat(b_conv.reshape(seqs, groups, state_dim), heads // groups, axis=1)
    c_heads = jnp.repeat(c_conv.reshape(seqs, groups, state_dim), heads // groups, axis=1)
    step = jax.nn.softplus(dt_raw + dt_bias)
    decay = jnp.exp(-step * jnp.exp(a_log))
    state_next = (
        decay[:, :, None, None] * ssm_state
        + (step[:, :, None] * x_heads)[:, :, :, None] * b_heads[:, :, None, :]
    )
    readout = jnp.einsum("shpn,shn->shp", state_next, c_heads) + d_skip[None, :, None] * x_heads
    gated = readout.reshape(seqs, heads * head_dim) * jax.nn.silu(z_new.astype(jnp.float32))
    grouped = gated.reshape(seqs, groups, -1)
    grouped = grouped * lax.rsqrt(jnp.mean(grouped * grouped, axis=-1, keepdims=True) + epsilon)
    mixed_heads = (grouped.reshape(seqs, heads * head_dim) * group_gain).astype(jnp.bfloat16)
    return (mixed_heads, state_next, conv_x_next, conv_b_next, conv_c_next)


def body(
    tokens,
    ssm_state,
    conv_x,
    conv_b,
    conv_c,
    w_x,
    w_z,
    w_b,
    w_c,
    w_dt,
    dt_bias,
    a_log,
    d_skip,
    taps_x,
    taps_b,
    taps_c,
    norm1_gain,
    group_gain,
    w_out,
    norm2_gain,
    route_ids,
    route_weights,
    exp_gate,
    exp_up,
    exp_down,
    dense_gate,
    dense_up,
    dense_down,
    branch_gate,
):
    seqs = tokens.shape[0]
    model_width = tokens.shape[1]
    stream = tokens.astype(jnp.float32)
    normed = rms_rows(stream, norm1_gain).astype(jnp.bfloat16)
    x_proj = jnp.dot(normed, w_x, preferred_element_type=jnp.float32).astype(jnp.bfloat16)
    z_proj = jnp.dot(normed, w_z, preferred_element_type=jnp.float32).astype(jnp.bfloat16)
    b_proj = jnp.dot(normed, w_b, preferred_element_type=jnp.float32).astype(jnp.bfloat16)
    c_proj = jnp.dot(normed, w_c, preferred_element_type=jnp.float32).astype(jnp.bfloat16)
    local_heads = ssm_state.shape[1]
    dt_columns = lax.dynamic_slice_in_dim(w_dt, lax.axis_index("tp") * local_heads, local_heads, 1)
    dt_raw = jnp.dot(normed, dt_columns, preferred_element_type=jnp.float32)
    mixed_heads, state_next, conv_x_next, conv_b_next, conv_c_next = mixer_core(
        x_proj,
        z_proj,
        b_proj,
        c_proj,
        dt_raw,
        ssm_state,
        conv_x,
        conv_b,
        conv_c,
        dt_bias,
        a_log,
        d_skip,
        taps_x,
        taps_b,
        taps_c,
        group_gain,
    )
    partial_out = jnp.dot(mixed_heads, w_out, preferred_element_type=jnp.float32)
    quarter = model_width // lax.axis_size("tp")
    column = lax.axis_index("tp") * quarter
    summed = over_copies(partial_out.astype(jnp.bfloat16), "tp").astype(jnp.float32)
    residual = (stream + summed).astype(jnp.bfloat16)
    normed2 = rms_rows(residual.astype(jnp.float32), norm2_gain).astype(jnp.bfloat16)
    own_rows = lax.dynamic_slice_in_dim(residual, column, quarter, 1)
    experts_all = lax.axis_size(EP) * exp_gate.shape[0]
    top_count = route_ids.shape[1]
    capacity = min(seqs, max(2, 2 * seqs * top_count // experts_all))
    expert_iota = jnp.arange(experts_all, dtype=jnp.int32)
    matches = route_ids[:, :, None] == expert_iota[None, None, :]
    routed = jnp.sum(matches.astype(jnp.int32), axis=1)
    weight_of = jnp.sum(jnp.where(matches, route_weights[:, :, None], jnp.float32(0.0)), axis=1)
    ranked = jnp.cumsum(routed, axis=0) - routed
    slot_iota = jnp.arange(capacity, dtype=jnp.int32)
    slot_onehot = routed[:, :, None] * (ranked[:, :, None] == slot_iota[None, None, :]).astype(
        jnp.int32
    )
    dispatch = slot_onehot.reshape(seqs, experts_all * capacity).astype(jnp.bfloat16)
    outgoing = jnp.einsum(
        "sk,sd->kd", dispatch, normed2, preferred_element_type=jnp.float32
    ).astype(jnp.bfloat16)
    outgoing = outgoing.reshape(experts_all, capacity, model_width)
    arrived = lax.all_to_all(outgoing, EP, split_axis=0, concat_axis=0, tiled=True)
    arrived_rows = arrived.reshape(-1, model_width)
    gate_pre = jnp.dot(arrived_rows, exp_gate[0], preferred_element_type=jnp.float32)
    up_pre = jnp.dot(arrived_rows, exp_up[0], preferred_element_type=jnp.float32)
    active = (jax.nn.silu(gate_pre) * up_pre).astype(jnp.bfloat16)
    expert_partial = jnp.dot(active, exp_down[0], preferred_element_type=jnp.float32)
    expert_part = sum_at_owner(expert_partial.astype(jnp.bfloat16), "tp", 1).astype(jnp.bfloat16)
    returned = lax.all_to_all(
        expert_part.reshape(-1, capacity, quarter), EP, split_axis=0, concat_axis=0, tiled=True
    )
    combine = (weight_of[:, :, None] * slot_onehot.astype(jnp.float32)).reshape(
        seqs, experts_all * capacity
    )
    expert_sum = jnp.dot(
        combine, returned.reshape(experts_all * capacity, quarter).astype(jnp.float32)
    )
    pieces = sent_together((dense_gate, dense_up), EP, 0, 1)
    dense_pre = jnp.dot(normed2, pieces[0], preferred_element_type=jnp.float32)
    dense_lift = jnp.dot(normed2, pieces[1], preferred_element_type=jnp.float32)
    dense_active = (jax.nn.silu(dense_pre) * dense_lift).astype(jnp.bfloat16)
    dense_partial = jnp.dot(
        dense_active, gather_axes(dense_down, EP, (1, 0, 2), 1), preferred_element_type=jnp.float32
    )
    dense_out = sum_at_owner(dense_partial.astype(jnp.bfloat16), "tp", 1)
    branch = jax.nn.sigmoid(
        jnp.dot(normed2, branch_gate[:, None], preferred_element_type=jnp.float32)
    )
    mixed = (own_rows.astype(jnp.float32) + expert_sum + branch * dense_out).astype(jnp.bfloat16)
    return (mixed, state_next, conv_x_next, conv_b_next, conv_c_next)


def solution(mesh):
    finer = Mesh(mesh.devices.reshape(8, 4, 2, mesh.shape["tp"]), ("ep_0", "ep_1", "ep_2", "tp"))
    in_specs = (
        P(EP, None),
        P(EP, "tp", None, None),
        P(EP, None, "tp"),
        P(EP, None, "tp"),
        P(EP, None, "tp"),
        P(None, "tp"),
        P(None, "tp"),
        P(None, "tp"),
        P(None, "tp"),
        P(),
        P("tp"),
        P("tp"),
        P("tp"),
        P(None, "tp"),
        P(None, "tp"),
        P(None, "tp"),
        P(),
        P("tp"),
        P("tp", None),
        P(),
        P(EP, None),
        P(EP, None),
        P(EP, None, "tp"),
        P(EP, None, "tp"),
        P(EP, "tp", None),
        P(EP, "tp"),
        P(EP, "tp"),
        P("tp", EP),
        P(),
    )
    out_specs = (
        P(EP, "tp"),
        P(EP, "tp", None, None),
        P(EP, None, "tp"),
        P(EP, None, "tp"),
        P(EP, None, "tp"),
    )
    return jax.shard_map(body, mesh=finer, in_specs=in_specs, out_specs=out_specs, check_vma=False)
```

profile of v0, /device:TPU:1, one launch (start us, length us, event | category | flops | bytes accessed | tf_op | source)
XLA Modules:
  0.0 136.8 jit_solution(10138319470427091095)
XLA Ops:
  7.3 1.4 %pad_maximum_fusion.3 = bf16[16,512]{1,0:T(8,128)(2,1)} fusion(bf16[16,256]{1,0:T(8,128)(2,1)} %param.55, bf16[16,256]{1,0:T(8,128)(2,1)} %param.54), kind=kLoop, calls=%fused_computation.78 | loop fusion | flops 32768 | bytes 32768 | tf_op jit(solution)/shard_map/concatenate | solution.py:40
  8.7 0.8 fusion.31
  9.5 0.7 convert_element_type.101
  10.2 1.3 fusion.7
  11.5 0.7 multiply_reduce_fusion.2
  12.3 0.7 exp.43
  12.9 1.5 %fusion.2 = bf16[8,1,512]{2,0,1:T(8,128)(2,1)S(1)} fusion(bf16[1024,512]{1,0:T(8,128)(2,1)} %param.34, bf16[8,1024]{1,0:T(8,128)(2,1)} %param.29, f32[1024]{0:T(1024)} %param.45, f32[8]{0:T(128)S(1)} %add_rsqrt_fusion.2), kind=kOutput, calls=%fused_computation.10 | convolution fusion | flops 8425472 | bytes 1077280 | tf_op jit(solution)/shard_map/dot_general | solution.py:149
  14.5 0.7 convert_element_type.98
  15.2 0.7 multiply_reduce_fusion
  16.0 1.3 fusion.8
  17.4 0.9 multiply_exponential_fusion
  18.4 2.0 %multiply_add_fusion = f32[8,8,64,128]{3,2,1,0:T(8,128)S(1)} fusion(f32[8,8,64,128]{3,2,1,0:T(8,128)} %param.30, f32[8,8,128]{2,1,0:T(8,128)S(1)} %bitcast.85, f32[8,8,64]{2,1,0:T(8,128)S(1)} %broadcast_multiply_fusion, f32[8,8]{1,0:T(8,128)S(1)} %get-tuple-element.7), kind=kLoop, calls=%fused_computation | loop fusion | flops 1572864 | bytes 4243712 | tf_op jit(solution)/shard_map/add | solution.py:103
  20.5 0.6 fusion.75
  21.8 1.5 %convolution_convert_fusion.2 = bf16[8,1024]{1,0:T(8,128)(2,1)S(1)} fusion(bf16[512,1024]{1,0:T(8,128)(2,1)} %param.47, f32[8,512]{1,0:T(8,128)S(1)} %get-tuple-element.10, f32[8,512]{1,0:T(8,128)S(1)} %bitcast.90, f32[512]{0:T(512)S(1)} %copy-done.14), kind=kOutput, calls=%fused_computation.5 | convolution fusion | flops 8409088 | bytes 1099776 | tf_op jit(solution)/shard_map/dot_general | solution.py:174
  24.0 4.8 %all-to-all-start = ((bf16[4,8,1024]{2,1,0:T(8,128)(2,1)}), bf16[4,8,1024]{2,1,0:T(8,128)(2,1)S(1)}, u32[]{:S(2)}, u32[]{:S(2)}) async-start(bf16[4,8,1024]{2,1,0:T(8,128)(2,1)} %broadcast_in_dim.27), calls=%async_computation | async-start | bytes 131072 | tf_op jit(solution)/shard_map/all_to_all | solution.py:15
  29.3 3.9 %all-to-all-done = bf16[4,8,1024]{2,1,0:T(8,128)(2,1)S(1)} async-done(((bf16[4,8,1024]{2,1,0:T(8,128)(2,1)}), bf16[4,8,1024]{2,1,0:T(8,128)(2,1)S(1)}, u32[]{:S(2)}, u32[]{:S(2)}) %all-to-all-start) | async-done | bytes 65568 | tf_op jit(solution)/shard_map/all_to_all | solution.py:15
  33.8 0.8 reshape.129
  34.6 13.9 %all-to-all-start.1 = ((bf16[64,2,1024]{2,1,0:T(2,128)(2,1)}), bf16[64,2,1024]{2,1,0:T(2,128)(2,1)S(1)}, u32[]{:S(2)}, u32[]{:S(2)}) async-start(bf16[64,2,1024]{2,1,0:T(2,128)(2,1)} %reshape.129), calls=%async_computation.1 | async-start | bytes 524288 | tf_op jit(solution)/shard_map/all_to_all | solution.py:198
  48.5 10.4 %all-gather = bf16[1024,16]{0,1:T(8,128)(2,1)S(1)} all-gather(bf16[256,16]{0,1:T(8,128)(2,1)S(1)} %copy-done.11), channel_id=2, replica_groups=mesh['ep_0'=8,'ep_1'=4,'ep_2'=2,'tp'=4] {'ep_1'}, dimensions={0}, use_global_device_ids=true | all-gather | bytes 40960 | tf_op jit(solution)/shard_map/all_gather | solution.py:53
  58.9 21.6 %all_gather.14 = bf16[32,256,16]{1,2,0:T(8,128)(2,1)S(1)} all-gather(bf16[4,256,16]{1,2,0:T(8,128)(2,1)S(1)} %bitcast.87), channel_id=1, replica_groups=mesh['ep_0'=8,'ep_1'=4,'ep_2'=2,'tp'=4] {'ep_0'}, dimensions={0}, use_global_device_ids=true | all-gather | bytes 294912 | tf_op jit(solution)/shard_map/all_gather | solution.py:53
  80.4 8.9 %all_gather.15 = bf16[64,256,16]{1,2,0:T(8,128)(2,1)S(1)} all-gather(bf16[32,256,16]{1,2,0:T(8,128)(2,1)S(1)} %all_gather.14), channel_id=1, replica_groups=mesh['ep_0'=8,'ep_1'=4,'ep_2'=2,'tp'=4] {'ep_2'}, dimensions={0}, use_global_device_ids=true | all-gather | bytes 786432 | tf_op jit(solution)/shard_map/all_gather | solution.py:53
  90.9 0.7 copy.83
  91.6 3.4 %all-to-all-start.2 = ((bf16[4,128,256]{2,1,0:T(8,128)(2,1)}), bf16[4,128,256]{2,1,0:T(8,128)(2,1)S(1)}, u32[]{:S(2)}, u32[]{:S(2)}) async-start(bf16[4,128,256]{2,1,0:T(8,128)(2,1)} %bitcast.77), calls=%async_computation.2 | async-start | bytes 524288 | tf_op jit(solution)/shard_map/all_to_all | solution.py:31
  95.1 1.2 fusion.15
  96.3 2.2 %convolution_convert_fusion.3 = bf16[8,1024]{1,0:T(8,128)(2,1)} fusion(bf16[256,1024]{0,1:T(8,128)(2,1)S(1)} %bitcast.79, bf16[1024,512]{1,0:T(8,128)(2,1)} %all-gather.3.cloned.1.call-done, f32[8,256]{1,0:T(8,128)S(1)} %fusion.15, bf16[8,1024]{1,0:T(8,128)(2,1)S(1)} %get-tuple-element.6, f32[1024]{0:T(1024)S(1)} %copy-done.10, f32[8]{0:T(128)S(1)} %add_rsqrt_fusion.1), kind=kOutput, calls=%fused_computation.6 | convolution fusion | flops 8441856 | bytes 1093664 | tf_op jit(solution)/shard_map/dot_general | solution.py:218
  98.5 2.6 %all-to-all-done.2 = bf16[4,128,256]{2,1,0:T(8,128)(2,1)S(1)} async-done(((bf16[4,128,256]{2,1,0:T(8,128)(2,1)}), bf16[4,128,256]{2,1,0:T(8,128)(2,1)S(1)}, u32[]{:S(2)}, u32[]{:S(2)}) %all-to-all-start.2) | async-done | bytes 262176 | tf_op jit(solution)/shard_map/all_to_all | solution.py:31
  101.1 3.2 %all-to-all-start.4 = ((bf16[4,8,256]{2,1,0:T(8,128)(2,1)}), bf16[4,8,256]{2,1,0:T(8,128)(2,1)S(1)}, u32[]{:S(2)}, u32[]{:S(2)}) async-start(bf16[4,8,256]{2,1,0:T(8,128)(2,1)} %bitcast.25), calls=%async_computation.4 | async-start | bytes 32768 | tf_op jit(solution)/shard_map/all_to_all | solution.py:31
  105.1 0.7 reshape.132
  105.7 2.8 %all-to-all-done.4 = bf16[4,8,256]{2,1,0:T(8,128)(2,1)S(1)} async-done(((bf16[4,8,256]{2,1,0:T(8,128)(2,1)}), bf16[4,8,256]{2,1,0:T(8,128)(2,1)S(1)}, u32[]{:S(2)}, u32[]{:S(2)}) %all-to-all-start.4) | async-done | bytes 16416 | tf_op jit(solution)/shard_map/all_to_all | solution.py:31
  108.5 10.5 %all-to-all-start.3 = ((bf16[64,2,256]{2,1,0:T(2,128)(2,1)}), bf16[64,2,256]{2,1,0:T(2,128)(2,1)S(1)}, u32[]{:S(2)}, u32[]{:S(2)}) async-start(bf16[64,2,256]{2,1,0:T(2,128)(2,1)} %reshape.132), calls=%async_computation.3 | async-start | bytes 131072 | tf_op jit(solution)/shard_map/all_to_all | solution.py:205
  119.3 9.9 %all-to-all-done.3 = bf16[64,2,256]{2,1,0:T(2,128)(2,1)S(1)} async-done(((bf16[64,2,256]{2,1,0:T(2,128)(2,1)}), bf16[64,2,256]{2,1,0:T(2,128)(2,1)S(1)}, u32[]{:S(2)}, u32[]{:S(2)}) %all-to-all-start.3) | async-done | bytes 65568 | tf_op jit(solution)/shard_map/all_to_all | solution.py:205
  129.1 0.8 fusion.5
  (87 shorter events, 5.0 us)
Async XLA Ops:
  7.2 14.2 %copy-start = (bf16[1024,512]{1,0:T(8,128)(2,1)S(1)}, bf16[1024,512]{1,0:T(8,128)(2,1)}, u32[]{:S(2)}) copy-start(bf16[1024,512]{1,0:T(8,128)(2,1)} %param.35) | copy-start | bytes 3145732
  7.2 10.2 %copy-start.2 = (bf16[8,1024]{1,0:T(8,128)(2,1)S(1)}, bf16[8,1024]{1,0:T(8,128)(2,1)}, u32[]{:S(2)}) copy-start(bf16[8,1024]{1,0:T(8,128)(2,1)} %param.29) | copy-start | bytes 49156
  7.2 10.2 %copy-start.7 = (f32[1024]{0:T(1024)S(1)}, f32[1024]{0:T(1024)}, u32[]{:S(2)}) copy-start(f32[1024]{0:T(1024)} %param.45) | copy-start | bytes 12292
  7.2 10.1 %copy-start.15 = (bf16[4,256]{1,0:T(4,128)(2,1)S(1)}, bf16[4,256]{1,0:T(4,128)(2,1)}, u32[]{:S(2)}) copy-start(bf16[4,256]{1,0:T(4,128)(2,1)} %param.44) | copy-start | bytes 6148
  7.2 10.1 %copy-start.9 = (bf16[8,3,256]{2,0,1:T(8,128)(2,1)S(1)}, bf16[8,3,256]{2,0,1:T(8,128)(2,1)}, u32[]{:S(2)}) copy-start(bf16[8,3,256]{2,0,1:T(8,128)(2,1)} %param.33) | copy-start | bytes 36868
  7.2 10.2 %copy-start.18 = (f32[8]{0:T(128)S(1)}, f32[8]{0:T(128)}, u32[]{:S(2)}) copy-start(f32[8]{0:T(128)} %param.39) | copy-start | bytes 100
  7.2 87.8 %all-gather.3.cloned.1.call-start = ((), (), s32[]{:S(2)}) async-start(), calls=%async_computation.5 | async-start | bytes 1064960 | tf_op jit(solution)/shard_map/all_gather | solution.py:41
  20.5 2.8 %copy-start.1 = (f32[8,8,64,128]{3,2,1,0:T(8,128)}, f32[8,8,64,128]{3,2,1,0:T(8,128)S(1)}, u32[]{:S(2)}) copy-start(f32[8,8,64,128]{3,2,1,0:T(8,128)S(1)} %multiply_add_fusion) | copy-start | bytes 6291460
  20.5 0.7 copy-start.17
  20.5 1.3 copy-start.14
  20.5 8.3 %copy-start.12 = (s32[8,6]{1,0:T(8,128)S(1)}, s32[8,6]{1,0:T(8,128)}, u32[]{:S(2)}) copy-start(s32[8,6]{1,0:T(8,128)} %param.49) | copy-start | bytes 580
  21.2 12.3 %copy-start.10 = (f32[1024]{0:T(1024)S(1)}, f32[1024]{0:T(1024)}, u32[]{:S(2)}) copy-start(f32[1024]{0:T(1024)} %param.48) | copy-start | bytes 12292
  21.4 27.1 %copy-start.11 = (bf16[256,16]{0,1:T(8,128)(2,1)S(1)}, bf16[256,16]{0,1:T(8,128)(2,1)}, u32[]{:S(2)}) copy-start(bf16[256,16]{0,1:T(8,128)(2,1)} %param.56) | copy-start | bytes 24580
  24.0 9.3 %all-to-all-start = ((bf16[4,8,1024]{2,1,0:T(8,128)(2,1)}), bf16[4,8,1024]{2,1,0:T(8,128)(2,1)S(1)}, u32[]{:S(2)}, u32[]{:S(2)}) async-start(bf16[4,8,1024]{2,1,0:T(8,128)(2,1)} %broadcast_in_dim.27), calls=%async_computation | async-start | bytes 131072 | tf_op jit(solution)/shard_map/all_to_all | solution.py:15
  29.1 60.3 %copy-start.13 = (f32[8,6]{1,0:T(8,128)S(1)}, f32[8,6]{1,0:T(8,128)}, u32[]{:S(2)}) copy-start(f32[8,6]{1,0:T(8,128)} %param.50) | copy-start | bytes 580
  29.1 60.4 %copy-start.6 = (bf16[8,3,512]{2,0,1:T(8,128)(2,1)S(1)}, bf16[8,3,512]{2,0,1:T(8,128)(2,1)}, u32[]{:S(2)}) copy-start(bf16[8,3,512]{2,0,1:T(8,128)(2,1)} %param.31) | copy-start | bytes 73732
  33.5 56.8 %copy-start.5 = (bf16[1,1024,128]{2,1,0:T(8,128)(2,1)S(1)}, bf16[1,1024,128]{2,1,0:T(8,128)(2,1)}, u32[]{:S(2)}) copy-start(bf16[1,1024,128]{2,1,0:T(8,128)(2,1)} %param.51) | copy-start | bytes 786436
  34.6 55.9 %copy-start.3 = (bf16[1,128,1024]{2,1,0:T(8,128)(2,1)S(1)}, bf16[1,128,1024]{2,1,0:T(8,128)(2,1)}, u32[]{:S(2)}) copy-start(bf16[1,128,1024]{2,1,0:T(8,128)(2,1)} %param.53) | copy-start | bytes 786436
  34.6 55.9 %copy-start.4 = (bf16[1,1024,128]{2,1,0:T(8,128)(2,1)S(1)}, bf16[1,1024,128]{2,1,0:T(8,128)(2,1)}, u32[]{:S(2)}) copy-start(bf16[1,1024,128]{2,1,0:T(8,128)(2,1)} %param.52) | copy-start | bytes 786436
  34.6 55.5 %all-to-all-start.1 = ((bf16[64,2,1024]{2,1,0:T(2,128)(2,1)}), bf16[64,2,1024]{2,1,0:T(2,128)(2,1)S(1)}, u32[]{:S(2)}, u32[]{:S(2)}) async-start(bf16[64,2,1024]{2,1,0:T(2,128)(2,1)} %reshape.129), calls=%async_computation.1 | async-start | bytes 524288 | tf_op jit(solution)/shard_map/all_to_all | solution.py:198
  90.3 14.1 %copy-start.8 = (bf16[8,3,256]{2,0,1:T(8,128)(2,1)S(1)}, bf16[8,3,256]{2,0,1:T(8,128)(2,1)}, u32[]{:S(2)}) copy-start(bf16[8,3,256]{2,0,1:T(8,128)(2,1)} %param.32) | copy-start | bytes 36868
  90.5 14.5 %copy-start.16 = (bf16[1024]{0:T(1024)(128)(2,1)S(1)}, bf16[1024]{0:T(1024)(128)(2,1)}, u32[]{:S(2)}) copy-start(bf16[1024]{0:T(1024)(128)(2,1)} %param.57) | copy-start | bytes 6148
  91.6 9.5 %all-to-all-start.2 = ((bf16[4,128,256]{2,1,0:T(8,128)(2,1)}), bf16[4,128,256]{2,1,0:T(8,128)(2,1)S(1)}, u32[]{:S(2)}, u32[]{:S(2)}) async-start(bf16[4,128,256]{2,1,0:T(8,128)(2,1)} %bitcast.77), calls=%async_computation.2 | async-start | bytes 524288 | tf_op jit(solution)/shard_map/all_to_all | solution.py:31
  101.1 7.4 %all-to-all-start.4 = ((bf16[4,8,256]{2,1,0:T(8,128)(2,1)}), bf16[4,8,256]{2,1,0:T(8,128)(2,1)S(1)}, u32[]{:S(2)}, u32[]{:S(2)}) async-start(bf16[4,8,256]{2,1,0:T(8,128)(2,1)} %bitcast.25), calls=%async_computation.4 | async-start | bytes 32768 | tf_op jit(solution)/shard_map/all_to_all | solution.py:31
  108.5 20.6 %all-to-all-start.3 = ((bf16[64,2,256]{2,1,0:T(2,128)(2,1)}), bf16[64,2,256]{2,1,0:T(2,128)(2,1)S(1)}, u32[]{:S(2)}, u32[]{:S(2)}) async-start(bf16[64,2,256]{2,1,0:T(2,128)(2,1)} %reshape.132), calls=%async_computation.3 | async-start | bytes 131072 | tf_op jit(solution)/shard_map/all_to_all | solution.py:205
Sparse Core Ops, SparseCore 0:
  10.8 81.2 all-gather.2
where the time goes:
time: 138 us; the launch traced here: 137 us
  blocking collectives  40.8 us (30%)
  starting transfers between devices  35.9 us (26%)
  waiting for transfers between devices  19.3 us (14%)
  between operations  14.5 us (11%)
  matrix products  12.7 us (9%)
  other arithmetic  9.06 us (7%)
  local copies, waits for them, and re-layouts  4.54 us (3%)
    all_gather x3, blocking collectives, all_blocks(): pieces = lax.all_gather(pieces, axes[k], axis=0, tiled=True)  40.8 us
    all_to_all x1, starting transfers between devices, body(): lax.all_to_all(outgoing, EP, split_axis=0, concat_axis=0, tiled=True)  13.9 us
    all_to_all x1, starting transfers between devices, body(): lax.all_to_all(expert_part.reshape(-1, capacity, quarter), EP, split_axis...  10.5 us
    all_to_all x1, waiting for transfers between devices, body(): lax.all_to_all(expert_part.reshape(-1, capacity, quarter), EP, split_axis...  9.88 us
    all_to_all x2, starting transfers between devices, sum_at_owner(): lax.all_to_all(pieces, axis, split_axis=0, concat_axis=0, tiled=True)  6.64 us
    all_to_all x2, waiting for transfers between devices, sum_at_owner(): lax.all_to_all(pieces, axis, split_axis=0, concat_axis=0, tiled=True)  5.44 us
    all_to_all x1, starting transfers between devices, copy_for_each(): lax.all_to_all(jnp.broadcast_to(shard[None], (size, *shard.shape)), axis,...  4.83 us
    all_to_all x1, waiting for transfers between devices, copy_for_each(): lax.all_to_all(jnp.broadcast_to(shard[None], (size, *shard.shape)), axis,...  3.94 us
  transfers between devices with their start and end apart: 6, of which 4 were waited for; matrix products, arithmetic and copies ran while one was open for 18% of the time, Pallas kernels for 0%

commit v1 on v0

v1 whole, which is shorter than its diff:
```python
import functools

import jax
import jax.numpy as jnp
from jax import lax
from jax.experimental import pallas as pl
from jax.experimental.pallas import tpu as pltpu
from jax.sharding import PartitionSpec as P

EPS = 1e-06
F32 = jnp.float32
BF16 = jnp.bfloat16
HIGH = lax.Precision.HIGHEST
MESH = pl.DeviceIdType.MESH


def dot(a, b, **kw):
    return jnp.dot(a, b, preferred_element_type=F32, **kw)


def dot_nt(a, b, **kw):
    return lax.dot_general(a, b, (((1,), (1,)), ((), ())), preferred_element_type=F32, **kw)


def iota(shape, dim):
    return lax.broadcasted_iota(jnp.int32, shape, dim)


def rms_rows(values, gain):
    return values * lax.rsqrt(jnp.mean(values * values, axis=-1, keepdims=True) + EPS) * gain


def silu(v):
    return v * jax.nn.sigmoid(v)


def mixer_kernel(
    tokens, state, conv_x, conv_b, conv_c, w_x, w_z, w_b, w_c, w_dt, dt_bias, a_log, d_skip, taps_x, taps_b, taps_c, gain,
    state_out, cx_out, cb_out, cc_out, y_out, z_out,
    st, vx, vz, vb, vc, wsem, isem, osem,
):
    seqs, heads, hd, sd = state.shape
    per = heads * sd // vb.shape[1]
    groups = heads // per
    loads = [pltpu.make_async_copy(src, dst, wsem.at[i]) for i, (src, dst) in enumerate(((w_x, vx), (w_b, vb), (w_c, vc), (w_z, vz)))]
    for c in loads:
        c.start()
    ins = [pltpu.make_async_copy(state.at[s], st.at[s], isem.at[s]) for s in range(seqs)]
    for c in ins:
        c.start()
    normed = rms_rows(tokens[...].astype(F32), gain[...]).astype(BF16)
    width = heads * hd
    me = lax.axis_index("tp")
    raw = dot_nt(normed, w_dt[...])
    all_heads = raw.shape[1]
    spread_all = (iota((all_heads, width), 0) == me * heads + iota((all_heads, width), 1) // hd).astype(F32)
    spread = (iota((heads, width), 0) == iota((heads, width), 1) // hd).astype(F32)
    raw = dot(raw, spread_all, precision=HIGH)
    bias = dot(dt_bias[...], spread, precision=HIGH)
    rate = jnp.exp(dot(a_log[...], spread, precision=HIGH))
    skip = dot(d_skip[...], spread, precision=HIGH)
    pre = raw + bias
    step = jnp.maximum(pre, 0.0) + jnp.log1p(jnp.exp(-jnp.abs(pre)))
    decay = jnp.exp(-step * rate)

    def conv(prev, fresh, taps, out):
        fresh = fresh.astype(BF16)
        tap = taps[...].astype(F32)
        depth = prev.shape[0]
        total = fresh.astype(F32) * tap[depth : depth + 1]
        for j in range(depth):
            total = total + prev[j].astype(F32) * tap[j : j + 1]
            out[j] = prev[j + 1] if j + 1 < depth else fresh
        return silu(total)

    loads[0].wait()
    xs = conv(conv_x, dot(normed, vx[...]), taps_x, cx_out)
    loads[1].wait()
    bs = conv(conv_b, dot(normed, vb[...]), taps_b, cb_out)
    loads[2].wait()
    cs = conv(conv_c, dot(normed, vc[...]), taps_c, cc_out)
    loads[3].wait()
    z_out[...] = dot(normed, vz[...]).astype(BF16).astype(F32)
    in_col = (step * xs).T
    decay_col = decay.T
    rows = per * hd
    lane = iota((rows, seqs), 1)
    reads = [jnp.zeros((rows, seqs), F32) for _ in range(groups)]
    outs = []
    for s in range(seqs):
        ins[s].wait()
        for g in range(groups):
            cut = slice(g * rows, (g + 1) * rows)
            old = st[s, g * per : (g + 1) * per].reshape(rows, sd)
            new = decay_col[cut, s : s + 1] * old + in_col[cut, s : s + 1] * bs[s : s + 1, g * sd : (g + 1) * sd]
            st[s, g * per : (g + 1) * per] = new.reshape(per, hd, sd)
            got = jnp.sum(new * cs[s : s + 1, g * sd : (g + 1) * sd], axis=1, keepdims=True)
            reads[g] = jnp.where(lane == s, got, reads[g])
        c = pltpu.make_async_copy(st.at[s], state_out.at[s], osem.at[s])
        c.start()
        outs.append(c)
    y_out[...] = jnp.concatenate(reads, axis=0).T + skip * xs
    for c in outs:
        c.wait()


PHASES = ("dense", "route", "part", "tok", "slot", "pre", "act", "exp", "dout", "ret", "comb")


def branch_kernel(
    NZ, NC, NT, n_groups,
    tokens, y_in, z_in, ggain, w_out, gain2, ids, wts, w_g, w_u, w_d, dgate, dup, ddown, bgate,
    mixed,
    vo, vg, vu, vd,
    dw, rt, pt, tk, bs_, br, cs_, cr, ac, xs_, xr, fs_, fr, gs_, gr, hs_, hr,
    ssem, rsem, lsem,
):
    S, D = tokens.shape
    inner = y_in.shape[1]
    quarter = D // NT
    planes = NZ // NT
    slots = 2 * NC
    E = NZ * NC
    e = lax.axis_index("ep")
    t = lax.axis_index("tp")
    z = e // NC
    yc = lax.rem(e, NC)
    q_mine = z // planes
    f_self = q_mine == t

    loads = [pltpu.make_async_copy(src, dst, lsem.at[i]) for i, (src, dst) in enumerate(((w_out, vo), (w_g.at[0], vg), (w_u.at[0], vu), (w_d.at[0], vd)))]
    for c in loads:
        c.start()

    zs = [lax.rem(z + d, NZ) for d in range(1, NZ)]
    cores = [lax.rem(yc + d, NC) for d in range(1, NC)]
    ts = [lax.rem(t + d, NT) for d in range(1, NT)]
    barrier = pltpu.get_barrier_semaphore()

    def greet(dev):
        pl.semaphore_signal(barrier, inc=1, device_id=dev, device_id_type=MESH)

    for p in zs:
        greet((p * NC + yc, t))
    for p in cores:
        greet((z * NC + p, t))
    for p in ts:
        greet((e, p))
    for a in range(planes):
        for b in range(NT):
            other_z = t * planes + a

            @pl.when(jnp.logical_or(other_z != z, b != t))
            def _():
                greet((other_z * NC + yc, b))

    sent = []

    def send(phase, src, dst, dev, slot):
        i = PHASES.index(phase)
        c = pltpu.make_async_remote_copy(
            src_ref=src, dst_ref=dst, send_sem=ssem.at[i, len([1 for s in sent if s[0] == i])], recv_sem=rsem.at[i, slot], device_id=dev, device_id_type=MESH
        )
        c.start()
        sent.append((i, c))

    def arrive(phase, ref, slot):
        i = PHASES.index(phase)
        pltpu.make_async_copy(ref.at[slot], ref.at[slot], rsem.at[i, slot]).wait()

    dw[yc] = jnp.concatenate([dgate[...].astype(F32), dup[...].astype(F32), ddown[...].astype(F32)], axis=1).astype(BF16)
    lane = iota((S, 2 * E), 1)
    named = jnp.zeros((S, 2 * E), F32)
    weight = jnp.zeros((S, 2 * E), F32)
    for k in range(ids.shape[1]):
        hit = ids[:, k : k + 1] == lane // 2
        named = jnp.where(hit, 1.0, named)
        weight = jnp.where(hit, wts[:, k : k + 1], weight)
    before = (iota((S, S), 0) > iota((S, S), 1)).astype(F32)
    rank = dot(before, named)
    mine = jnp.logical_and(named > 0.5, jnp.abs(rank - lax.rem(lane, 2).astype(F32)) < 0.5)
    rt[z] = jnp.concatenate([jnp.where(mine, 1.0, 0.0), jnp.where(mine, weight, 0.0)], axis=1).astype(BF16)

    gated = y_in[...] * silu(z_in[...])
    width = inner // n_groups
    parts = []
    for g in range(inner // width):
        v = gated[:, g * width : (g + 1) * width]
        parts.append(v * lax.rsqrt(jnp.mean(v * v, axis=-1, keepdims=True) + EPS) * ggain[:, g * width : (g + 1) * width])
    heads = jnp.concatenate(parts, axis=1).astype(BF16)
    loads[0].wait()
    pt[t] = dot(heads, vo[...]).astype(BF16)

    n_wait = (NZ - 1) + (NC - 1) + (NT - 1) + NZ
    pl.semaphore_wait(barrier, n_wait - f_self.astype(jnp.int32))

    for p in ts:
        send("part", pt.at[t], pt.at[t], (e, p), t)
    for p in zs:
        send("route", rt.at[z], rt.at[z], (p * NC + yc, t), z)
    for p in cores:
        send("dense", dw.at[yc], dw.at[yc], (z * NC + p, t), yc)

    for p in ts:
        arrive("part", pt, p)
    total = pt[0].astype(F32)
    for k in range(1, NT):
        total = total + pt[k].astype(F32)
    residual = (tokens[...].astype(F32) + total).astype(BF16).astype(F32)
    normed = rms_rows(residual, gain2[...]).astype(BF16)
    tk[z] = normed
    for p in zs:
        send("tok", tk.at[z], tk.at[z], (p * NC + yc, t), z)
    lanes = bgate.shape[1]
    weighted = jnp.zeros((S, lanes), F32)
    for k in range(bgate.shape[0]):
        weighted = weighted + normed[:, k * lanes : (k + 1) * lanes].astype(F32) * bgate[k : k + 1, :].astype(F32)
    branch = jax.nn.sigmoid(jnp.sum(weighted, axis=1, keepdims=True))
    own = jnp.zeros((S, quarter), F32)
    for k in range(NT):
        own = jnp.where(t == k, residual[:, k * quarter : (k + 1) * quarter], own)

    for p in zs:
        arrive("route", rt, p)
    routes = jnp.concatenate([rt[k].astype(F32) for k in range(NZ)], axis=0)
    R = NC * NZ * 2
    row, col = iota((R, 2 * E), 0), iota((R, 2 * E), 1)
    pick = (col == z * slots + 2 * (row // (2 * NZ)) + lax.rem(row, 2)).astype(BF16)
    same = lax.rem(iota((R, NZ * S), 0) // 2, NZ) == iota((R, NZ * S), 1) // S
    take = jnp.where(same, dot_nt(pick, routes[:, : 2 * E].astype(BF16)), 0.0).astype(BF16)
    same_t = lax.rem(iota((NZ * S, R), 1) // 2, NZ) == iota((NZ * S, R), 0) // S
    give = jnp.where(same_t, dot_nt(routes[:, 2 * E :].astype(BF16), pick), 0.0).astype(BF16)

    for p in zs:
        arrive("tok", tk, p)
    toks = jnp.concatenate([tk[k].astype(F32) for k in range(NZ)], axis=0).astype(BF16)
    bs_[...] = dot(take, toks).astype(BF16).reshape(bs_.shape)
    for p in cores:
        send("slot", bs_.at[p], br.at[yc], (z * NC + p, t), yc)
    br[yc] = bs_[yc]

    for p in cores:
        arrive("dense", dw, p)
    depth = D // NZ
    cut = pl.ds(pl.multiple_of(z * depth, depth), depth)
    mine_cols = jnp.concatenate([tk[k, :, cut].astype(F32) for k in range(NZ)], axis=0).astype(BF16)
    hid = dw.shape[2] // 3
    plane_w = jnp.concatenate([dw[k] for k in range(NC)], axis=0)
    cs_[...] = dot(mine_cols, plane_w[:, : 2 * hid]).astype(BF16).astype(F32).reshape(NZ, S, 2 * hid).astype(BF16)
    for p in zs:
        send("pre", cs_.at[p], cr.at[z], (p * NC + yc, t), z)
    cr[z] = cs_[z]
    for p in zs:
        arrive("pre", cr, p)
    pre = cr[0].astype(F32)
    for k in range(1, NZ):
        pre = pre + cr[k].astype(F32)
    ac[z] = (silu(pre[:, :hid]) * pre[:, hid:]).astype(BF16)
    for p in zs:
        send("act", ac.at[z], ac.at[z], (p * NC + yc, t), z)

    for c in loads[1:]:
        c.wait()
    for p in cores:
        arrive("slot", br, p)
    rows_in = br[...].reshape(R, D)
    active = (silu(dot(rows_in, vg[...])) * dot(rows_in, vu[...])).astype(BF16)
    for k in range(NT):
        xs_[k] = dot(active, vd[:, k * quarter : (k + 1) * quarter]).astype(BF16)
    for p in ts:
        send("exp", xs_.at[p], xr.at[t], (e, p), t)
    xr[t] = xs_[t]

    for p in zs:
        arrive("act", ac, p)
    acts = jnp.concatenate([ac[k].astype(F32) for k in range(NZ)], axis=0).astype(BF16)
    fs_[...] = dot_nt(acts, plane_w[:, 2 * hid :]).reshape(fs_.shape).astype(BF16)
    f_slot = lax.rem(z, planes) * NT + t
    i = PHASES.index("dout")
    f_copies = []
    for k in range(NZ):
        there = jnp.logical_or(z != k, jnp.logical_not(f_self))
        c = pltpu.make_async_remote_copy(
            src_ref=fs_.at[k], dst_ref=fr.at[f_slot], send_sem=ssem.at[i, k], recv_sem=rsem.at[i, f_slot], device_id=(k * NC + yc, q_mine), device_id_type=MESH
        )
        f_copies.append((there, c))

        @pl.when(there)
        def _():
            c.start()

    @pl.when(f_self)
    def _():
        fr[f_slot] = fs_[z]

    for p in ts:
        arrive("exp", xr, p)
    summed = xr[0].astype(F32)
    for k in range(1, NT):
        summed = summed + xr[k].astype(F32)
    gs_[...] = summed.astype(BF16).reshape(gs_.shape)
    for p in cores:
        send("ret", gs_.at[p], gr.at[yc], (z * NC + p, t), yc)
    gr[yc] = gs_[yc]
    for p in cores:
        arrive("ret", gr, p)
    hs_[...] = dot(give, gr[...].reshape(R, quarter)).reshape(hs_.shape).astype(BF16)
    for p in zs:
        send("comb", hs_.at[p], hr.at[z], (p * NC + yc, t), z)
    hr[z] = hs_[z]

    for a in range(planes):
        for b in range(NT):
            slot = a * NT + b

            @pl.when(jnp.logical_or(t * planes + a != z, b != t))
            def _():
                arrive("dout", fr, slot)

    dense = []
    for a in range(planes):
        v = fr[a * NT].astype(F32)
        for b in range(1, NT):
            v = v + fr[a * NT + b].astype(F32)
        dense.append(v)
    dense = jnp.concatenate(dense, axis=1)
    for p in zs:
        arrive("comb", hr, p)
    expert = hr[0].astype(F32)
    for k in range(1, NZ):
        expert = expert + hr[k].astype(F32)
    mixed[...] = (own + expert + branch * dense).astype(BF16)
    for _, c in sent:
        c.wait_send()
    for there, c in f_copies:

        @pl.when(there)
        def _():
            c.wait_send()


def body(
    tokens, ssm_state, conv_x, conv_b, conv_c, w_x, w_z, w_b, w_c, w_dt, dt_bias, a_log, d_skip, taps_x, taps_b, taps_c,
    norm1_gain, group_gain, w_out, norm2_gain, route_ids, route_weights, exp_gate, exp_up, exp_down, dense_gate, dense_up, dense_down, branch_gate,
    *, NZ, NC, NT, sd,
):
    S, D = tokens.shape
    heads, hd = ssm_state.shape[1:3]
    inner = w_x.shape[1]
    cols = w_b.shape[1]
    vm, hbm = pl.BlockSpec(memory_space=pltpu.VMEM), pl.BlockSpec(memory_space=pl.ANY)
    dma = pltpu.SemaphoreType.DMA
    state_next, cx, cb, cc, y, zz = pl.pallas_call(
        mixer_kernel,
        name="mixer",
        out_shape=(
            jax.ShapeDtypeStruct(ssm_state.shape, F32),
            jax.ShapeDtypeStruct((3, S, inner), BF16),
            jax.ShapeDtypeStruct((3, S, cols), BF16),
            jax.ShapeDtypeStruct((3, S, cols), BF16),
            jax.ShapeDtypeStruct((S, inner), F32),
            jax.ShapeDtypeStruct((S, inner), F32),
        ),
        in_specs=[vm, hbm, vm, vm, vm, hbm, hbm, hbm, hbm] + [vm] * 8,
        out_specs=(hbm, vm, vm, vm, vm, vm),
        scratch_shapes=[
            pltpu.VMEM(ssm_state.shape, F32),
            pltpu.VMEM((D, inner), BF16),
            pltpu.VMEM((D, inner), BF16),
            pltpu.VMEM((D, cols), BF16),
            pltpu.VMEM((D, cols), BF16),
            dma((4,)),
            dma((S,)),
            dma((S,)),
        ],
        compiler_params=pltpu.CompilerParams(vmem_limit_bytes=60_000_000),
    )(
        tokens, ssm_state, turned(conv_x), turned(conv_b), turned(conv_c), w_x, w_z, w_b, w_c, w_dt.T, dt_bias[None], a_log[None], d_skip[None], taps_x, taps_b, taps_c, norm1_gain[None]
    )
    quarter = D // NT
    hidden, dhid = exp_gate.shape[2], dense_gate.shape[1]
    R = NZ * NC * 2
    mixed = pl.pallas_call(
        functools.partial(branch_kernel, NZ, NC, NT, cols // sd),
        name="branches",
        out_shape=jax.ShapeDtypeStruct((S, quarter), BF16),
        in_specs=[vm, vm, vm, vm, hbm, vm, vm, vm, hbm, hbm, hbm, vm, vm, vm, vm],
        out_specs=vm,
        scratch_shapes=[
            pltpu.VMEM((inner, D), BF16),
            pltpu.VMEM((D, hidden), BF16),
            pltpu.VMEM((D, hidden), BF16),
            pltpu.VMEM((hidden, D), BF16),
            pltpu.VMEM((NC, dense_gate.shape[0], 3 * dhid), BF16),
            pltpu.VMEM((NZ, S, 4 * NZ * NC), BF16),
            pltpu.VMEM((NT, S, D), BF16),
            pltpu.VMEM((NZ, S, D), BF16),
            pltpu.VMEM((NC, 2 * NZ, D), BF16),
            pltpu.VMEM((NC, 2 * NZ, D), BF16),
            pltpu.VMEM((NZ, S, 2 * dhid), BF16),
            pltpu.VMEM((NZ, S, 2 * dhid), BF16),
            pltpu.VMEM((NZ, S, dhid), BF16),
            pltpu.VMEM((NT, R, quarter), BF16),
            pltpu.VMEM((NT, R, quarter), BF16),
            pltpu.VMEM((NZ, S, D // NZ), BF16),
            pltpu.VMEM((NZ, S, D // NZ), BF16),
            pltpu.VMEM((NC, 2 * NZ, quarter), BF16),
            pltpu.VMEM((NC, 2 * NZ, quarter), BF16),
            pltpu.VMEM((NZ, S, quarter), BF16),
            pltpu.VMEM((NZ, S, quarter), BF16),
            dma((len(PHASES), max(NZ, NC, NT))),
            dma((len(PHASES), max(NZ, NC, NT))),
            dma((4,)),
        ],
        compiler_params=pltpu.CompilerParams(collective_id=0, has_side_effects=True, vmem_limit_bytes=60_000_000),
    )(
        tokens, y, zz, group_gain[None], w_out, norm2_gain[None], route_ids, route_weights,
        exp_gate, exp_up, exp_down, dense_gate, dense_up, dense_down.T, branch_gate.reshape(D // 128, 128),
    )
    return mixed, state_next, turned(cx), turned(cb), turned(cc)


def turned(a):
    return jnp.transpose(a, (1, 0, 2))


def solution(mesh):
    NT = mesh.shape["tp"]
    NC = 8 if mesh.shape["ep"] >= 64 else 2
    NZ = mesh.shape["ep"] // NC
    ep = P("ep", None)
    in_specs = (
        ep, P("ep", "tp", None, None), P("ep", None, "tp"), P("ep", None, "tp"), P("ep", None, "tp"),
        P(None, "tp"), P(None, "tp"), P(None, "tp"), P(None, "tp"), P(), P("tp"), P("tp"), P("tp"),
        P(None, "tp"), P(None, "tp"), P(None, "tp"), P(), P("tp"), P("tp", None), P(), ep, ep,
        P("ep", None, "tp"), P("ep", None, "tp"), P("ep", "tp", None), P("ep", "tp"), P("ep", "tp"), P("tp", "ep"), P(),
    )
    out_specs = (P("ep", "tp"), P("ep", "tp", None, None), P("ep", None, "tp"), P("ep", None, "tp"), P("ep", None, "tp"))
    part = functools.partial(body, NZ=NZ, NC=NC, NT=NT, sd=128)
    return jax.shard_map(part, mesh=mesh, in_specs=in_specs, out_specs=out_specs, check_vma=False)
```

time: 138 us -> 53.1 us (0.38)
  Pallas kernels: 0 us -> 50.9 us
  blocking collectives: 40.8 us -> 0 us
  starting transfers between devices: 35.9 us -> 0 us
  waiting for transfers between devices: 19.3 us -> 0 us
  between operations: 14.5 us -> 0.65 us
  matrix products: 12.7 us -> 0 us
  other arithmetic: 9.06 us -> 0 us
  local copies, waits for them, and re-layouts: 4.54 us -> 1.27 us
    pallas_call x0 -> x2, Pallas kernels: none -> 50.9 us  [the longest x1 42.2 us: body(): pl.pallas_call(functools.partial(branch_kernel, NZ, NC, NT, cols // sd),...]
    all_gather x3 -> x0, blocking collectives: 40.8 us -> none  [all_blocks(): pieces = lax.all_gather(pieces, axes[k], axis=0, tiled=True)]
    all_to_all x5 -> x0, starting transfers between devices: 35.9 us -> none  [the longest x1 13.9 us: body(): lax.all_to_all(outgoing, EP, split_axis=0, concat_axis=0, tiled=True)]
    all_to_all x5 -> x0, waiting for transfers between devices: 19.3 us -> none  [the longest x1 9.88 us: body(): lax.all_to_all(expert_part.reshape(-1, capacity, quarter), EP, split_axis...]
    dot_general x14 -> x0, matrix products: 12.7 us -> none  [the longest x1 2.19 us: body(): jnp.dot(dense_active, gather_axes(dense_down, EP, (1, 0, 2), 1), preferre...]
    reduce_sum x11 -> x0, other arithmetic: 2.76 us -> none  [the longest x3 1.49 us: short_conv(): jnp.sum(window.astype(jnp.float32) * taps.astype(jnp.float32)[None], axis=1)]
    concatenate x3 -> x0, other arithmetic: 2.61 us -> none  [the longest x1 1.38 us: sent_together(): both = jnp.concatenate(arrays, axis=along)]
    reshape x5 -> x0, local copies, waits for them, and re-layouts: 2.36 us -> none  [the longest x1 0.81 us: body(): outgoing = outgoing.reshape(experts_all, capacity, model_width)]
  transfers between devices with their start and end apart: 6 -> 0, of which waited for: 4 -> 0; matrix products, arithmetic and copies ran while one was open for 18% -> 0% of each run, Pallas kernels for 0% -> 0%
where the time goes in v1:
time: 53.1 us; the launch traced here: 52.8 us
  Pallas kernels  50.9 us (96%)
  local copies, waits for them, and re-layouts  1.27 us (2%)
  between operations  0.65 us (1%)
    pallas_call x1, Pallas kernels, body(): pl.pallas_call(functools.partial(branch_kernel, NZ, NC, NT, cols // sd),...  42.2 us
    pallas_call x1, Pallas kernels, body(): pl.pallas_call(mixer_kernel, name='mixer', out_shape=(jax.ShapeDtypeStruc...  8.65 us
    unnamed x1, local copies, waits for them, and re-layouts  1.27 us

profile of v1, /device:TPU:1, one launch (start us, length us, event | category | flops | bytes accessed | tf_op | source)
XLA Modules:
  0.0 52.8 jit_solution(7932599660943515940)
XLA Ops:
  0.6 8.7 %mixer.1 = (f32[8,8,64,128]{3,2,1,0:T(8,128)}, bf16[3,8,512]{2,1,0:T(8,128)(2,1)}, bf16[3,8,256]{2,1,0:T(8,128)(2,1)}, bf16[3,8,256]{2,1,0:T(8,128)(2,1)}, f32[8,512]{1,0:T(8,128)}, /*index=5*/f32[8,512]{1,0:T(8,128)}) custom-call(bf16[8,1024]{1,0:T(8,128)(2,1)} %tokens.3, f32[8,8,64,128]{3,2,1,0:T(8,128)} %state.1, bf16[3,8,512]{2,1,0:T(8,128)(2,1)} %bitcast.16, ...), custom_call_target="tpu_custom_call" | custom-call | tf_op jit(solution)/shard_map/mixer/pallas_call | solution.py:353
  9.3 42.2 %branches.1 = bf16[8,256]{1,0:T(8,128)(2,1)} custom-call(bf16[8,1024]{1,0:T(8,128)(2,1)} %tokens.3, f32[8,512]{1,0:T(8,128)} %get-tuple-element.11.y_in, f32[8,512]{1,0:T(8,128)} %get-tuple-element.12.z_in, f32[1,512]{1,0:T(1,128)} %bitcast.22, bf16[512,1024]{1,0:T(8,128)(2,1)} %w_out.1, f32[1,1024]{1,0:T(1,128)} %bitcast.20, s32[8,6]{1,0:T(8,128)} %ids.1, ...), custom_call_target="tpu_custom_call" | custom-call | tf_op jit(solution)/shard_map/branches/pallas_call | solution.py:383
  51.6 1.3 %copy.35 = bf16[8,256]{1,0:T(8,128)(2,1)} copy(bf16[8,256]{1,0:T(8,128)(2,1)} %branches.1) | data formatting | bytes 8192

commit v2 on v1

v2 whole, which is shorter than its diff:
```python
import functools

import jax
import jax.numpy as jnp
from jax import lax
from jax.experimental import pallas as pl
from jax.experimental.pallas import tpu as pltpu
from jax.sharding import PartitionSpec as P

EPS = 1e-06
F32 = jnp.float32
BF16 = jnp.bfloat16
HIGH = lax.Precision.HIGHEST
MESH = pl.DeviceIdType.MESH
VMEM_STEP = 24_000_000
VMEM_STORE = 4_000_000


def dot(a, b, **kw):
    return jnp.dot(a, b, preferred_element_type=F32, **kw)


def dot_nt(a, b, **kw):
    return lax.dot_general(a, b, (((1,), (1,)), ((), ())), preferred_element_type=F32, **kw)


def iota(shape, dim):
    return lax.broadcasted_iota(jnp.int32, shape, dim)


def rms_rows(values, gain):
    return values * lax.rsqrt(jnp.mean(values * values, axis=-1, keepdims=True) + EPS) * gain


def silu(v):
    return v * jax.nn.sigmoid(v)


def step_kernel(NE, NC, NT, n_groups, *refs):
    given, refs = refs[:20], refs[20:]
    state, w_x, w_z, w_b, w_c, w_out, w_g, w_u, w_d = refs[:9]
    mixed, state_out, cx_out, cb_out, cc_out = refs[9:14]
    small, refs = refs[14:34], refs[34:]
    tokens, conv_x, conv_b, conv_c, w_dt, dt_bias, a_log, d_skip, taps_x, taps_b, taps_c, gain = small[:12]
    ggain, gain2, ids, wts, dgate, dup, ddown, bgate = small[12:]
    vx, vz, vb, vc, st, vo, vg, vu, vd, pt, dw, dq, tk, cs_, cr, ac, bs_, br, aa, fs_, fr, dout, gs_, gr, lsem, isem, tsem, ssem, rsem = refs
    NZ = NE // NC
    S, D = tokens.shape
    heads, hd, sd = st.shape[1:]
    inner = heads * hd
    per = heads // n_groups
    quarter = D // NT
    planes = NZ // NT
    R = 2 * NE
    e = lax.axis_index("ep")
    t = lax.axis_index("tp")
    z = e // NC
    yc = lax.rem(e, NC)
    q_mine = z // planes
    f_self = q_mine == t

    loads = {}
    for i, (name, src, dst) in enumerate((
        ("x", w_x, vx), ("b", w_b, vb), ("c", w_c, vc), ("z", w_z, vz), ("o", w_out, vo), ("d", w_d.at[0], vd), ("g", w_g.at[0], vg), ("u", w_u.at[0], vu)
    )):
        loads[name] = pltpu.make_async_copy(src, dst, lsem.at[i])
    tiny = [pltpu.make_async_copy(src, dst, tsem.at[i]) for i, (src, dst) in enumerate(zip(given, small))]
    for c in tiny[:12]:
        c.start()
    for name in "xbc":
        loads[name].start()
    ins = [pltpu.make_async_copy(state.at[s], st.at[s], isem.at[s]) for s in range(S)]
    for c in ins:
        c.start()
    for name in "zo":
        loads[name].start()
    for c in tiny[12:]:
        c.start()
    for name in "dgu":
        loads[name].start()

    barrier = pltpu.get_barrier_semaphore()

    def greet(dev):
        pl.semaphore_signal(barrier, inc=1, device_id=dev, device_id_type=MESH)

    def each_ep(count, start):
        def one(k, c):
            half = (k + 1) // 2
            start(lax.rem(e + count // 2 + (1 - 2 * lax.rem(k, 2)) * half, count))
            return c

        lax.fori_loop(0, count - 1, one, 0)

    each_ep(NE, lambda p: greet((p, t)))
    ts = [lax.rem(t + d, NT) for d in range(1, NT)]
    zs = [lax.rem(z + d, NZ) for d in (NZ // 2, *[d for d in range(1, NZ) if d != NZ // 2])]
    cores = [lax.rem(yc + d, NC) for d in range(1, NC)]
    for p in ts:
        greet((e, p))
    for a in range(planes):
        for b in range(NT):
            other_z = t * planes + a

            @pl.when(jnp.logical_or(other_z != z, b != t))
            def _():
                greet((other_z * NC + yc, b))

    PART, DENSE, DOWN, COLS, PRE, ACT, SLOT, HID, DOUT, RET = range(10)

    def send(i, src, dst, dev):
        pltpu.make_async_remote_copy(src_ref=src, dst_ref=dst, send_sem=ssem.at[i], recv_sem=rsem.at[i], device_id=dev, device_id_type=MESH).start()

    def wait(sem, ref, count):
        pltpu.make_async_copy(ref.at[pl.ds(0, count)], ref.at[pl.ds(0, count)], sem).wait()

    def arrive(i, ref, count):
        wait(rsem.at[i], ref, count)

    for c in tiny[:12]:
        c.wait()
    normed = rms_rows(tokens[...].astype(F32), gain[...]).astype(BF16)
    raw = dot_nt(normed, w_dt[...])
    total_heads = raw.shape[1]
    spread_all = (iota((total_heads, inner), 0) == t * heads + iota((total_heads, inner), 1) // hd).astype(F32)
    spread = (iota((heads, inner), 0) == iota((heads, inner), 1) // hd).astype(F32)
    raw = dot(raw, spread_all, precision=HIGH)
    bias = dot(dt_bias[...], spread, precision=HIGH)
    rate = jnp.exp(dot(a_log[...], spread, precision=HIGH))
    skip = dot(d_skip[...], spread, precision=HIGH)
    pre = raw + bias
    step = jnp.maximum(pre, 0.0) + jnp.log1p(jnp.exp(-jnp.abs(pre)))
    decay = jnp.exp(-step * rate)

    def conv(prev, fresh, taps, out):
        fresh = fresh.astype(BF16)
        tap = taps[...].astype(F32)
        depth = prev.shape[0]
        total = fresh.astype(F32) * tap[depth : depth + 1]
        for j in range(depth):
            total = total + prev[j].astype(F32) * tap[j : j + 1]
            out[j] = prev[j + 1] if j + 1 < depth else fresh
        return silu(total)

    loads["x"].wait()
    xs = conv(conv_x, dot(normed, vx[...]), taps_x, cx_out)
    loads["b"].wait()
    bs = conv(conv_b, dot(normed, vb[...]), taps_b, cb_out)
    loads["c"].wait()
    cs = conv(conv_c, dot(normed, vc[...]), taps_c, cc_out)
    inflow = step * xs
    rows = per * hd
    lane = iota((rows, S), 1)
    reads = [jnp.zeros((rows, S), F32) for _ in range(n_groups)]
    for s in range(S):
        ins[s].wait()
        for g in range(n_groups):
            old = st[s, g * per : (g + 1) * per].reshape(rows, sd)
            got = jnp.sum(old * cs[s : s + 1, g * sd : (g + 1) * sd], axis=1, keepdims=True)
            reads[g] = jnp.where(lane == s, got, reads[g])
    loads["z"].wait()
    zz = dot(normed, vz[...]).astype(BF16).astype(F32)
    both = [jnp.sum(bs[:, g * sd : (g + 1) * sd] * cs[:, g * sd : (g + 1) * sd], axis=1, keepdims=True) for g in range(n_groups)]
    for c in tiny[12:]:
        c.wait()
    parts = []
    for g in range(n_groups):
        cut = slice(g * rows, (g + 1) * rows)
        v = decay[:, cut] * reads[g].T + inflow[:, cut] * both[g] + skip[:, cut] * xs[:, cut]
        v = v * silu(zz[:, cut])
        parts.append(v * lax.rsqrt(jnp.mean(v * v, axis=-1, keepdims=True) + EPS) * ggain[:, cut])
    mixed_heads = jnp.concatenate(parts, axis=1).astype(BF16)
    loads["o"].wait()
    pt[t] = dot(mixed_heads, vo[...]).astype(BF16)

    pl.semaphore_wait(barrier, (NE - 1) + (NT - 1) + NZ - f_self.astype(jnp.int32))
    for p in ts:
        send(PART, pt.at[t], pt.at[t], (e, p))
    dw[yc] = jnp.concatenate([dgate[...].astype(F32), dup[...].astype(F32), ddown[...].astype(F32)], axis=1).astype(BF16)
    for p in cores:
        send(DENSE, dw.at[yc], dw.at[yc], (z * NC + p, t))
    loads["d"].wait()
    for p in ts:
        send(DOWN, vd.at[:, pl.ds(pl.multiple_of(p * quarter, quarter), quarter)], dq.at[t], (e, p))
    dq[t] = vd[:, pl.ds(pl.multiple_of(t * quarter, quarter), quarter)]

    slot = iota((S, R), 1)
    named = jnp.zeros((S, R), F32)
    weight = jnp.zeros((S, R), F32)
    for k in range(ids.shape[1]):
        hit = ids[:, k : k + 1] == slot // 2
        named = jnp.where(hit, 1.0, named)
        weight = jnp.where(hit, wts[:, k : k + 1], weight)
    before = (iota((S, S), 0) > iota((S, S), 1)).astype(F32)
    rank = dot(before, named)
    mine = jnp.logical_and(named > 0.5, jnp.abs(rank - lax.rem(slot, 2).astype(F32)) < 0.5)
    take = jnp.where(mine, 1.0, 0.0).T.astype(BF16)
    give = jnp.where(mine, weight, 0.0)

    arrive(PART, pt, NT - 1)
    total = pt[0].astype(F32)
    for k in range(1, NT):
        total = total + pt[k].astype(F32)
    residual = (tokens[...].astype(F32) + total).astype(BF16).astype(F32)
    normed2 = rms_rows(residual, gain2[...]).astype(BF16)
    bs_[...] = dot(take, normed2).astype(BF16).reshape(bs_.shape)
    each_ep(NE, lambda p: send(SLOT, bs_.at[p], br.at[e], (p, t)))
    br[e] = bs_[e]
    depth = D // NZ
    for k in range(NZ):
        fr[k] = normed2[:, k * depth : (k + 1) * depth]
    for p in zs:
        send(COLS, fr.at[p], tk.at[z], (p * NC + yc, t))
    tk[z] = fr[z]

    in_col = inflow.T
    decay_col = decay.T
    for s in range(S):
        for g in range(n_groups):
            cut = slice(g * rows, (g + 1) * rows)
            old = st[s, g * per : (g + 1) * per].reshape(rows, sd)
            new = decay_col[cut, s : s + 1] * old + in_col[cut, s : s + 1] * bs[s : s + 1, g * sd : (g + 1) * sd]
            state_out[s, g * per : (g + 1) * per] = new.reshape(per, hd, sd)

    lanes = bgate.shape[1]
    weighted = jnp.zeros((S, lanes), F32)
    for k in range(bgate.shape[0]):
        weighted = weighted + normed2[:, k * lanes : (k + 1) * lanes].astype(F32) * bgate[k : k + 1, :].astype(F32)
    branch = jax.nn.sigmoid(jnp.sum(weighted, axis=1, keepdims=True))
    own = jnp.zeros((S, quarter), F32)
    for k in range(NT):
        own = jnp.where(t == k, residual[:, k * quarter : (k + 1) * quarter], own)

    def stacked(ref, count):
        return jnp.concatenate([ref[k].astype(F32) for k in range(count)], axis=0).astype(BF16)

    arrive(DENSE, dw, NC - 1)
    arrive(COLS, tk, NZ - 1)
    hid = dw.shape[2] // 3
    plane_w = jnp.concatenate([dw[k] for k in range(NC)], axis=0)
    cs_[...] = dot(stacked(tk, NZ), plane_w[:, : 2 * hid]).reshape(cs_.shape).astype(BF16)
    for p in zs:
        send(PRE, cs_.at[p], cr.at[z], (p * NC + yc, t))
    cr[z] = cs_[z]
    arrive(PRE, cr, NZ - 1)
    pre = cr[0].astype(F32)
    for k in range(1, NZ):
        pre = pre + cr[k].astype(F32)
    ac[z] = (silu(pre[:, :hid]) * pre[:, hid:]).astype(BF16)
    for p in zs:
        send(ACT, ac.at[z], ac.at[z], (p * NC + yc, t))

    loads["g"].wait()
    loads["u"].wait()
    arrive(SLOT, br, NE - 1)
    arrived = br[...].reshape(R, D)
    aa[t] = (silu(dot(arrived, vg[...])) * dot(arrived, vu[...])).astype(BF16)
    for p in ts:
        send(HID, aa.at[t], aa.at[t], (e, p))

    arrive(ACT, ac, NZ - 1)
    wait(ssem.at[COLS], fr, NZ - 1)
    fs_[...] = dot_nt(stacked(ac, NZ), plane_w[:, 2 * hid :]).reshape(fs_.shape).astype(BF16)
    f_slot = lax.rem(z, planes) * NT + t

    def give_dense(k, c):
        @pl.when(jnp.logical_or(z != k, q_mine != t))
        def _():
            send(DOUT, fs_.at[k], dout.at[f_slot], (k * NC + yc, q_mine))

        return c

    lax.fori_loop(0, NZ, give_dense, 0)

    @pl.when(f_self)
    def _():
        dout[f_slot] = fs_[z]

    arrive(DOWN, dq, NT - 1)
    arrive(HID, aa, NT - 1)
    hidden = jnp.concatenate([aa[k] for k in range(NT)], axis=1)
    down = jnp.concatenate([dq[k] for k in range(NT)], axis=0)
    gs_[...] = dot(hidden, down).astype(BF16).reshape(gs_.shape)
    each_ep(NE, lambda p: send(RET, gs_.at[p], gr.at[e], (p, t)))
    gr[e] = gs_[e]

    @pl.when(f_self)
    def _():
        arrive(DOUT, dout, NZ - 1)

    @pl.when(jnp.logical_not(f_self))
    def _():
        arrive(DOUT, dout, NZ)

    dense = []
    for a in range(planes):
        v = dout[a * NT].astype(F32)
        for b in range(1, NT):
            v = v + dout[a * NT + b].astype(F32)
        dense.append(v)
    base = own + branch * jnp.concatenate(dense, axis=1)
    arrive(RET, gr, NE - 1)
    mixed[...] = (base + dot(give.astype(BF16), gr[...].reshape(R, quarter))).astype(BF16)

    for i, ref, count in ((PART, pt, NT - 1), (DENSE, dw, NC - 1), (DOWN, dq, NT - 1), (PRE, cs_, NZ - 1), (ACT, ac, NZ - 1), (SLOT, bs_, NE - 1), (HID, aa, NT - 1), (RET, gs_, NE - 1)):
        wait(ssem.at[i], ref, count)

    @pl.when(f_self)
    def _():
        wait(ssem.at[DOUT], fs_, NZ - 1)

    @pl.when(jnp.logical_not(f_self))
    def _():
        wait(ssem.at[DOUT], fs_, NZ)


def store_kernel(count, *refs):
    ins, outs, sem = refs[:count], refs[count : 2 * count], refs[2 * count]
    copies = [pltpu.make_async_copy(a, b, sem.at[i]) for i, (a, b) in enumerate(zip(ins, outs))]
    for c in copies:
        c.start()
    for c in copies:
        c.wait()


def body(
    tokens, ssm_state, conv_x, conv_b, conv_c, w_x, w_z, w_b, w_c, w_dt, dt_bias, a_log, d_skip, taps_x, taps_b, taps_c,
    norm1_gain, group_gain, w_out, norm2_gain, route_ids, route_weights, exp_gate, exp_up, exp_down, dense_gate, dense_up, dense_down, branch_gate,
    *, NE, NC, NT, sd,
):
    S, D = tokens.shape
    NZ = NE // NC
    inner = w_x.shape[1]
    cols = w_b.shape[1]
    quarter = D // NT
    hidden, dhid = exp_gate.shape[2], dense_gate.shape[1]
    R = 2 * NE
    depth = D // NZ
    vm, hbm, free = (pl.BlockSpec(memory_space=m) for m in (pltpu.VMEM, pltpu.HBM, pl.ANY))
    dma = pltpu.SemaphoreType.DMA
    half = lambda *shape: pltpu.VMEM(shape, BF16)
    shape = jax.ShapeDtypeStruct
    small = (
        tokens, turned(conv_x), turned(conv_b), turned(conv_c), w_dt.T, dt_bias[None], a_log[None], d_skip[None], taps_x, taps_b, taps_c, norm1_gain[None],
        group_gain[None], norm2_gain[None], route_ids, route_weights, dense_gate, dense_up, dense_down.T, branch_gate.reshape(D // 128, 128),
    )
    made = pl.pallas_call(
        functools.partial(step_kernel, NE, NC, NT, cols // sd),
        name="step",
        out_shape=(
            shape((S, quarter), BF16), shape(ssm_state.shape, F32), shape((3, S, inner), BF16), shape((3, S, cols), BF16), shape((3, S, cols), BF16),
        ),
        in_specs=[hbm] * 29,
        out_specs=(vm,) * 5,
        scratch_shapes=[pltpu.VMEM(a.shape, a.dtype) for a in small]
        + [
            half(D, inner), half(D, inner), half(D, cols), half(D, cols), pltpu.VMEM(ssm_state.shape, F32),
            half(inner, D), half(D, hidden), half(D, hidden), half(hidden, D),
            half(NT, S, D), half(NC, dense_gate.shape[0], 3 * dhid), half(NT, hidden, quarter),
            half(NZ, S, depth), half(NZ, S, 2 * dhid), half(NZ, S, 2 * dhid), half(NZ, S, dhid),
            half(NE, 2, D), half(NE, 2, D), half(NT, R, hidden),
            half(NZ, S, depth), half(NZ, S, depth), half(NZ, S, depth),
            half(NE, 2, quarter), half(NE, 2, quarter),
            dma((8,)), dma((S,)), dma((20,)), dma((10,)), dma((10,)),
        ],
        compiler_params=pltpu.CompilerParams(collective_id=0, has_side_effects=True, vmem_limit_bytes=VMEM_STEP),
    )(
        *(fixed(a) for a in small),
        *(fixed(a) for a in (ssm_state, w_x, w_z, w_b, w_c, w_out, exp_gate, exp_up, exp_down)),
    )
    mixed, state_next, cx, cb, cc = pl.pallas_call(
        functools.partial(store_kernel, len(made)),
        name="store",
        out_shape=tuple(shape(a.shape, a.dtype) for a in made),
        in_specs=[free] * len(made),
        out_specs=(hbm,) * len(made),
        scratch_shapes=[dma((len(made),))],
        compiler_params=pltpu.CompilerParams(vmem_limit_bytes=VMEM_STORE),
    )(*made)
    return mixed, state_next, turned(cx), turned(cb), turned(cc)


def fixed(a):
    return pltpu.with_memory_space_constraint(a, pltpu.HBM)


def turned(a):
    return jnp.transpose(a, (1, 0, 2))


def solution(mesh):
    NT = mesh.shape["tp"]
    NC = 8 if mesh.shape["ep"] >= 64 else 2
    NE = mesh.shape["ep"]
    ep = P("ep", None)
    in_specs = (
        ep, P("ep", "tp", None, None), P("ep", None, "tp"), P("ep", None, "tp"), P("ep", None, "tp"),
        P(None, "tp"), P(None, "tp"), P(None, "tp"), P(None, "tp"), P(), P("tp"), P("tp"), P("tp"),
        P(None, "tp"), P(None, "tp"), P(None, "tp"), P(), P("tp"), P("tp", None), P(), ep, ep,
        P("ep", None, "tp"), P("ep", None, "tp"), P("ep", "tp", None), P("ep", "tp"), P("ep", "tp"), P("tp", "ep"), P(),
    )
    out_specs = (P("ep", "tp"), P("ep", "tp", None, None), P("ep", None, "tp"), P("ep", None, "tp"), P("ep", None, "tp"))
    part = functools.partial(body, NE=NE, NC=NC, NT=NT, sd=128)
    return jax.shard_map(part, mesh=mesh, in_specs=in_specs, out_specs=out_specs, check_vma=False)
```

time: 53.1 us -> 44 us (0.83)
  Pallas kernels: 50.9 us -> 43.3 us
  local copies, waits for them, and re-layouts: 1.27 us -> 0 us
    pallas_call x2, Pallas kernels: 50.9 us -> 43.3 us  [the longest x1 41.9 us: body(): pl.pallas_call(functools.partial(step_kernel, NE, NC, NT, cols // sd), na...]
    unnamed x1 -> x0, local copies, waits for them, and re-layouts: 1.27 us -> none
where the time goes in v2:
time: 44 us; the launch traced here: 43.9 us
  Pallas kernels  43.3 us (98%)
  between operations  0.65 us (1%)
    pallas_call x1, Pallas kernels, body(): pl.pallas_call(functools.partial(step_kernel, NE, NC, NT, cols // sd), na...  41.9 us
    pallas_call x1, Pallas kernels, body(): pl.pallas_call(functools.partial(store_kernel, len(made)), name='store',...  1.38 us

profile of v2, /device:TPU:1, one launch (start us, length us, event | category | flops | bytes accessed | tf_op | source)
XLA Modules:
  0.0 43.9 jit_solution(8427728358575738380)
XLA Ops:
  0.6 41.9 %step.1 = (bf16[8,256]{1,0:T(8,128)(2,1)S(1)}, f32[8,8,64,128]{3,2,1,0:T(8,128)S(1)}, bf16[3,8,512]{2,1,0:T(8,128)(2,1)S(1)}, bf16[3,8,256]{2,1,0:T(8,128)(2,1)S(1)}, bf16[3,8,256]{2,1,0:T(8,128)(2,1)S(1)}) custom-call(bf16[8,1024]{1,0:T(8,128)(2,1)} %refs_0_.1, bf16[3,8,512]{2,1,0:T(8,128)(2,1)} %bitcast.16, bf16[3,8,256]{2,1,0:T(8,128)(2,1)} %bitcast.17, ...), custom_call_target="tpu_custom_call" | custom-call | tf_op jit(solution)/shard_map/step/pallas_call | solution.py:347
  42.5 1.4 %store.1 = (bf16[8,256]{1,0:T(8,128)(2,1)}, f32[8,8,64,128]{3,2,1,0:T(8,128)}, bf16[3,8,512]{2,1,0:T(8,128)(2,1)}, bf16[3,8,256]{2,1,0:T(8,128)(2,1)}, bf16[3,8,256]{2,1,0:T(8,128)(2,1)}) custom-call(bf16[8,256]{1,0:T(8,128)(2,1)S(1)} %get-tuple-element.15.refs_0_, f32[8,8,64,128]{3,2,1,0:T(8,128)S(1)} %get-tuple-element.16.refs_1_, ...), custom_call_target="tpu_custom_call" | custom-call | tf_op jit(solution)/shard_map/store/pallas_call | solution.py:371

commit v3 on v2

--- a/solution.py
+++ b/solution.py
@@ -43,21 +43,18 @@
     small, refs = refs[14:34], refs[34:]
     tokens, conv_x, conv_b, conv_c, w_dt, dt_bias, a_log, d_skip, taps_x, taps_b, taps_c, gain = small[:12]
     ggain, gain2, ids, wts, dgate, dup, ddown, bgate = small[12:]
-    vx, vz, vb, vc, st, vo, vg, vu, vd, pt, dw, dq, tk, cs_, cr, ac, bs_, br, aa, fs_, fr, dout, gs_, gr, lsem, isem, tsem, ssem, rsem = refs
+    vx, vz, vb, vc, st, vo, vg, vu, vd, pt, d1, d2, d3, dq, tk, rt, bs_, br, aa, fs_, fr, gs_, gr, lsem, isem, tsem, ssem, rsem = refs
     NZ = NE // NC
     S, D = tokens.shape
     heads, hd, sd = st.shape[1:]
     inner = heads * hd
     per = heads // n_groups
     quarter = D // NT
-    planes = NZ // NT
     R = 2 * NE
     e = lax.axis_index("ep")
     t = lax.axis_index("tp")
     z = e // NC
     yc = lax.rem(e, NC)
-    q_mine = z // planes
-    f_self = q_mine == t
 
     loads = {}
     for i, (name, src, dst) in enumerate((
@@ -96,17 +93,11 @@
     ts = [lax.rem(t + d, NT) for d in range(1, NT)]
     zs = [lax.rem(z + d, NZ) for d in (NZ // 2, *[d for d in range(1, NZ) if d != NZ // 2])]
     cores = [lax.rem(yc + d, NC) for d in range(1, NC)]
-    for p in ts:
-        greet((e, p))
-    for a in range(planes):
-        for b in range(NT):
-            other_z = t * planes + a
-
-            @pl.when(jnp.logical_or(other_z != z, b != t))
-            def _():
-                greet((other_z * NC + yc, b))
-
-    PART, DENSE, DOWN, COLS, PRE, ACT, SLOT, HID, DOUT, RET = range(10)
+    for d in range(NZ):
+        for p in ts:
+            greet((lax.rem(z + d, NZ) * NC + yc, p))
+
+    PART, ROUTE, DENSE, DENSE2, DOWN, TOK, SLOT, DOUT, HID, RET = range(10)
 
     def send(i, src, dst, dev):
         pltpu.make_async_remote_copy(src_ref=src, dst_ref=dst, send_sem=ssem.at[i], recv_sem=rsem.at[i], device_id=dev, device_id_type=MESH).start()
@@ -173,16 +164,9 @@
     loads["o"].wait()
     pt[t] = dot(mixed_heads, vo[...]).astype(BF16)
 
-    pl.semaphore_wait(barrier, (NE - 1) + (NT - 1) + NZ - f_self.astype(jnp.int32))
+    pl.semaphore_wait(barrier, (NE - 1) + NZ * (NT - 1))
     for p in ts:
         send(PART, pt.at[t], pt.at[t], (e, p))
-    dw[yc] = jnp.concatenate([dgate[...].astype(F32), dup[...].astype(F32), ddown[...].astype(F32)], axis=1).astype(BF16)
-    for p in cores:
-        send(DENSE, dw.at[yc], dw.at[yc], (z * NC + p, t))
-    loads["d"].wait()
-    for p in ts:
-        send(DOWN, vd.at[:, pl.ds(pl.multiple_of(p * quarter, quarter), quarter)], dq.at[t], (e, p))
-    dq[t] = vd[:, pl.ds(pl.multiple_of(t * quarter, quarter), quarter)]
 
     slot = iota((S, R), 1)
     named = jnp.zeros((S, R), F32)
@@ -194,24 +178,27 @@
     before = (iota((S, S), 0) > iota((S, S), 1)).astype(F32)
     rank = dot(before, named)
     mine = jnp.logical_and(named > 0.5, jnp.abs(rank - lax.rem(slot, 2).astype(F32)) < 0.5)
-    take = jnp.where(mine, 1.0, 0.0).T.astype(BF16)
+    rt[z] = jnp.where(mine, 1.0, 0.0).astype(BF16)
     give = jnp.where(mine, weight, 0.0)
-
-    arrive(PART, pt, NT - 1)
-    total = pt[0].astype(F32)
-    for k in range(1, NT):
-        total = total + pt[k].astype(F32)
-    residual = (tokens[...].astype(F32) + total).astype(BF16).astype(F32)
-    normed2 = rms_rows(residual, gain2[...]).astype(BF16)
-    bs_[...] = dot(take, normed2).astype(BF16).reshape(bs_.shape)
-    each_ep(NE, lambda p: send(SLOT, bs_.at[p], br.at[e], (p, t)))
-    br[e] = bs_[e]
-    depth = D // NZ
+    hs = dgate.shape[1] // NZ
+    lane = iota((dgate.shape[0], 128), 1)
+    three = [dgate[...].astype(F32), dup[...].astype(F32), ddown[...].astype(F32)]
     for k in range(NZ):
-        fr[k] = normed2[:, k * depth : (k + 1) * depth]
+        page, off = k * hs // 128 * 128, k * hs % 128
+        block = jnp.zeros(lane.shape, F32)
+        for j, v in enumerate(three):
+            v = v[:, page : page + 128]
+            shift = (j * hs - off) % 128
+            block = jnp.where(jnp.logical_and(lane >= j * hs, lane < (j + 1) * hs), pltpu.roll(v, shift, 1) if shift else v, block)
+        d1[k] = block.astype(BF16)
     for p in zs:
-        send(COLS, fr.at[p], tk.at[z], (p * NC + yc, t))
-    tk[z] = fr[z]
+        send(ROUTE, rt.at[z], rt.at[z], (p * NC + yc, t))
+        send(DENSE, d1.at[p], d2.at[z], (p * NC + yc, t))
+    d2[z] = d1[z]
+    loads["d"].wait()
+    for p in ts:
+        send(DOWN, vd.at[:, pl.ds(pl.multiple_of(p * quarter, quarter), quarter)], dq.at[t], (e, p))
+    dq[t] = vd[:, pl.ds(pl.multiple_of(t * quarter, quarter), quarter)]
 
     in_col = inflow.T
     decay_col = decay.T
@@ -222,6 +209,22 @@
             new = decay_col[cut, s : s + 1] * old + in_col[cut, s : s + 1] * bs[s : s + 1, g * sd : (g + 1) * sd]
             state_out[s, g * per : (g + 1) * per] = new.reshape(per, hd, sd)
 
+    arrive(PART, pt, NT - 1)
+    total = pt[0].astype(F32)
+    for k in range(1, NT):
+        total = total + pt[k].astype(F32)
+    residual = (tokens[...].astype(F32) + total).astype(BF16).astype(F32)
+    normed2 = rms_rows(residual, gain2[...]).astype(BF16)
+    tk[z] = normed2
+    for p in zs:
+        send(TOK, tk.at[z], tk.at[z], (p * NC + yc, t))
+
+    arrive(DENSE, d2, NZ - 1)
+    for p in cores:
+        send(DENSE2, d2, d3.at[:, yc], (z * NC + p, t))
+    for k in range(NZ):
+        d3[k, yc] = d2[k]
+
     lanes = bgate.shape[1]
     weighted = jnp.zeros((S, lanes), F32)
     for k in range(bgate.shape[0]):
@@ -234,84 +237,61 @@
     def stacked(ref, count):
         return jnp.concatenate([ref[k].astype(F32) for k in range(count)], axis=0).astype(BF16)
 
-    arrive(DENSE, dw, NC - 1)
-    arrive(COLS, tk, NZ - 1)
-    hid = dw.shape[2] // 3
-    plane_w = jnp.concatenate([dw[k] for k in range(NC)], axis=0)
-    cs_[...] = dot(stacked(tk, NZ), plane_w[:, : 2 * hid]).reshape(cs_.shape).astype(BF16)
-    for p in zs:
-        send(PRE, cs_.at[p], cr.at[z], (p * NC + yc, t))
-    cr[z] = cs_[z]
-    arrive(PRE, cr, NZ - 1)
-    pre = cr[0].astype(F32)
-    for k in range(1, NZ):
-        pre = pre + cr[k].astype(F32)
-    ac[z] = (silu(pre[:, :hid]) * pre[:, hid:]).astype(BF16)
-    for p in zs:
-        send(ACT, ac.at[z], ac.at[z], (p * NC + yc, t))
+    arrive(ROUTE, rt, NZ - 1)
+    row, col = iota((R, R), 0), iota((R, R), 1)
+    pick = (col == z * 2 * NC + 2 * (row // (2 * NZ)) + lax.rem(row, 2)).astype(BF16)
+    same = lax.rem(iota((R, NZ * S), 0) // 2, NZ) == iota((R, NZ * S), 1) // S
+    take = jnp.where(same, dot_nt(pick, stacked(rt, NZ)), 0.0).astype(BF16)
+
+    arrive(TOK, tk, NZ - 1)
+    toks = stacked(tk, NZ)
+    bs_[...] = dot(take, toks).astype(BF16).reshape(bs_.shape)
+    for p in cores:
+        send(SLOT, bs_.at[p], br.at[yc], (z * NC + p, t))
+    br[yc] = bs_[yc]
+
+    arrive(DENSE2, d3, NZ * (NC - 1) // NC)
+    dense_w = d3[...].reshape(D, 128)
+    pre = dot(toks, dense_w)
+    act = silu(pltpu.roll(pre, 2 * hs, 1)) * pltpu.roll(pre, hs, 1)
+    lane = iota(act.shape, 1)
+    act = jnp.where(jnp.logical_and(lane >= 2 * hs, lane < 3 * hs), act, 0.0).astype(BF16)
+    out = dot_nt(act, dense_w)
+    for k in range(NZ):
+        for j in range(NT):
+            fs_[k * NT + j] = out[k * S : (k + 1) * S, j * quarter : (j + 1) * quarter].astype(BF16)
+    for d in range(1, NZ * NT):
+        p, q = lax.rem(z + d // NT, NZ), lax.rem(t + d % NT, NT)
+        send(DOUT, fs_.at[p * NT + q], fr.at[z * NT + t], (p * NC + yc, q))
+    fr[z * NT + t] = fs_[z * NT + t]
 
     loads["g"].wait()
     loads["u"].wait()
-    arrive(SLOT, br, NE - 1)
+    arrive(SLOT, br, NC - 1)
     arrived = br[...].reshape(R, D)
     aa[t] = (silu(dot(arrived, vg[...])) * dot(arrived, vu[...])).astype(BF16)
     for p in ts:
         send(HID, aa.at[t], aa.at[t], (e, p))
 
-    arrive(ACT, ac, NZ - 1)
-    wait(ssem.at[COLS], fr, NZ - 1)
-    fs_[...] = dot_nt(stacked(ac, NZ), plane_w[:, 2 * hid :]).reshape(fs_.shape).astype(BF16)
-    f_slot = lax.rem(z, planes) * NT + t
-
-    def give_dense(k, c):
-        @pl.when(jnp.logical_or(z != k, q_mine != t))
-        def _():
-            send(DOUT, fs_.at[k], dout.at[f_slot], (k * NC + yc, q_mine))
-
-        return c
-
-    lax.fori_loop(0, NZ, give_dense, 0)
-
-    @pl.when(f_self)
-    def _():
-        dout[f_slot] = fs_[z]
-
     arrive(DOWN, dq, NT - 1)
+    down = jnp.concatenate([dq[k] for k in range(NT)], axis=0)
     arrive(HID, aa, NT - 1)
     hidden = jnp.concatenate([aa[k] for k in range(NT)], axis=1)
-    down = jnp.concatenate([dq[k] for k in range(NT)], axis=0)
     gs_[...] = dot(hidden, down).astype(BF16).reshape(gs_.shape)
-    each_ep(NE, lambda p: send(RET, gs_.at[p], gr.at[e], (p, t)))
-    gr[e] = gs_[e]
-
-    @pl.when(f_self)
-    def _():
-        arrive(DOUT, dout, NZ - 1)
-
-    @pl.when(jnp.logical_not(f_self))
-    def _():
-        arrive(DOUT, dout, NZ)
-
-    dense = []
-    for a in range(planes):
-        v = dout[a * NT].astype(F32)
-        for b in range(1, NT):
-            v = v + dout[a * NT + b].astype(F32)
-        dense.append(v)
-    base = own + branch * jnp.concatenate(dense, axis=1)
+    each_ep(NE, lambda p: send(RET, gs_.at[lax.rem(p, NC) * NZ + p // NC], gr.at[e], (p, t)))
+    gr[e] = gs_[yc * NZ + z]
+
+    arrive(DOUT, fr, NZ * NT - 1)
+    dense = jnp.zeros((S, quarter), F32)
+    for k in range(NZ * NT):
+        dense = dense + fr[k].astype(F32)
+    base = own + branch * dense
     arrive(RET, gr, NE - 1)
     mixed[...] = (base + dot(give.astype(BF16), gr[...].reshape(R, quarter))).astype(BF16)
 
-    for i, ref, count in ((PART, pt, NT - 1), (DENSE, dw, NC - 1), (DOWN, dq, NT - 1), (PRE, cs_, NZ - 1), (ACT, ac, NZ - 1), (SLOT, bs_, NE - 1), (HID, aa, NT - 1), (RET, gs_, NE - 1)):
+    for i, ref, count in ((PART, pt, NT - 1), (ROUTE, rt, NZ - 1), (DENSE, d1, NZ - 1), (DENSE2, d3, NZ * (NC - 1) // NC), (DOWN, dq, NT - 1), (TOK, tk, NZ - 1), (SLOT, bs_, NC - 1), (HID, aa, NT - 1), (RET, gs_, NE - 1)):
         wait(ssem.at[i], ref, count)
-
-    @pl.when(f_self)
-    def _():
-        wait(ssem.at[DOUT], fs_, NZ - 1)
-
-    @pl.when(jnp.logical_not(f_self))
-    def _():
-        wait(ssem.at[DOUT], fs_, NZ)
+    wait(ssem.at[DOUT], fr, NZ * NT - 1)
 
 
 def store_kernel(count, *refs):
@@ -333,9 +313,9 @@
     inner = w_x.shape[1]
     cols = w_b.shape[1]
     quarter = D // NT
-    hidden, dhid = exp_gate.shape[2], dense_gate.shape[1]
+    hidden = exp_gate.shape[2]
     R = 2 * NE
-    depth = D // NZ
+    rows = dense_gate.shape[0]
     vm, hbm, free = (pl.BlockSpec(memory_space=m) for m in (pltpu.VMEM, pltpu.HBM, pl.ANY))
     dma = pltpu.SemaphoreType.DMA
     half = lambda *shape: pltpu.VMEM(shape, BF16)
@@ -356,10 +336,9 @@
         + [
             half(D, inner), half(D, inner), half(D, cols), half(D, cols), pltpu.VMEM(ssm_state.shape, F32),
             half(inner, D), half(D, hidden), half(D, hidden), half(hidden, D),
-            half(NT, S, D), half(NC, dense_gate.shape[0], 3 * dhid), half(NT, hidden, quarter),
-            half(NZ, S, depth), half(NZ, S, 2 * dhid), half(NZ, S, 2 * dhid), half(NZ, S, dhid),
-            half(NE, 2, D), half(NE, 2, D), half(NT, R, hidden),
-            half(NZ, S, depth), half(NZ, S, depth), half(NZ, S, depth),
+            half(NT, S, D), half(NZ, rows, 128), half(NZ, rows, 128), half(NZ, NC, rows, 128), half(NT, hidden, quarter),
+            half(NZ, S, D), half(NZ, S, R), half(NC, 2 * NZ, D), half(NC, 2 * NZ, D), half(NT, R, hidden),
+            half(NZ * NT, S, quarter), half(NZ * NT, S, quarter),
             half(NE, 2, quarter), half(NE, 2, quarter),
             dma((8,)), dma((S,)), dma((20,)), dma((10,)), dma((10,)),
         ],

time: 44 us -> 41 us (0.932)
  Pallas kernels: 43.3 us -> 40.3 us
    pallas_call x1, Pallas kernels: 41.9 us -> 38.9 us  [body(): pl.pallas_call(functools.partial(step_kernel, NE, NC, NT, cols // sd), na...]
where the time goes in v3:
time: 41 us; the launch traced here: 40.9 us
  Pallas kernels  40.3 us (98%)
  between operations  0.65 us (2%)
    pallas_call x1, Pallas kernels, body(): pl.pallas_call(functools.partial(step_kernel, NE, NC, NT, cols // sd), na...  38.9 us
    pallas_call x1, Pallas kernels, body(): pl.pallas_call(functools.partial(store_kernel, len(made)), name='store',...  1.38 us

profile of v3, /device:TPU:1, one launch (start us, length us, event | category | flops | bytes accessed | tf_op | source)
XLA Modules:
  0.0 40.9 jit_solution(6152456707401891776)
XLA Ops:
  0.6 38.9 %step.1 = (bf16[8,256]{1,0:T(8,128)(2,1)S(1)}, f32[8,8,64,128]{3,2,1,0:T(8,128)S(1)}, bf16[3,8,512]{2,1,0:T(8,128)(2,1)S(1)}, bf16[3,8,256]{2,1,0:T(8,128)(2,1)S(1)}, bf16[3,8,256]{2,1,0:T(8,128)(2,1)S(1)}) custom-call(bf16[8,1024]{1,0:T(8,128)(2,1)} %refs_0_.1, bf16[3,8,512]{2,1,0:T(8,128)(2,1)} %bitcast.16, bf16[3,8,256]{2,1,0:T(8,128)(2,1)} %bitcast.17, ...), custom_call_target="tpu_custom_call" | custom-call | tf_op jit(solution)/shard_map/step/pallas_call | solution.py:327
  39.6 1.4 %store.1 = (bf16[8,256]{1,0:T(8,128)(2,1)}, f32[8,8,64,128]{3,2,1,0:T(8,128)}, bf16[3,8,512]{2,1,0:T(8,128)(2,1)}, bf16[3,8,256]{2,1,0:T(8,128)(2,1)}, bf16[3,8,256]{2,1,0:T(8,128)(2,1)}) custom-call(bf16[8,256]{1,0:T(8,128)(2,1)S(1)} %get-tuple-element.15.refs_0_, f32[8,8,64,128]{3,2,1,0:T(8,128)S(1)} %get-tuple-element.16.refs_1_, ...), custom_call_target="tpu_custom_call" | custom-call | tf_op jit(solution)/shard_map/store/pallas_call | solution.py:350

commit v4 on v3

--- a/solution.py
+++ b/solution.py
@@ -91,16 +91,20 @@
 
     each_ep(NE, lambda p: greet((p, t)))
     ts = [lax.rem(t + d, NT) for d in range(1, NT)]
-    zs = [lax.rem(z + d, NZ) for d in (NZ // 2, *[d for d in range(1, NZ) if d != NZ // 2])]
+    ring = sorted(range(NZ), key=lambda d: (min(d, NZ - d), d))
+    half = NZ // 2
+    groups = (ring[:half], ring[half:])
+    at = [lax.rem(z + d, NZ) for d in range(NZ)]
+    zs = [at[d] for d in reversed(ring) if d]
     cores = [lax.rem(yc + d, NC) for d in range(1, NC)]
     for d in range(NZ):
         for p in ts:
             greet((lax.rem(z + d, NZ) * NC + yc, p))
 
-    PART, ROUTE, DENSE, DENSE2, DOWN, TOK, SLOT, DOUT, HID, RET = range(10)
-
-    def send(i, src, dst, dev):
-        pltpu.make_async_remote_copy(src_ref=src, dst_ref=dst, send_sem=ssem.at[i], recv_sem=rsem.at[i], device_id=dev, device_id_type=MESH).start()
+    PART, ROUTE, DENSE, DENSE2, DOWN, TOK, SLOT, DOUT, HID, RET, TOK2, SLOT2, HID2 = range(13)
+
+    def send(i, src, dst, dev, there=None):
+        pltpu.make_async_remote_copy(src_ref=src, dst_ref=dst, send_sem=ssem.at[i], recv_sem=rsem.at[i if there is None else there], device_id=dev, device_id_type=MESH).start()
 
     def wait(sem, ref, count):
         pltpu.make_async_copy(ref.at[pl.ds(0, count)], ref.at[pl.ds(0, count)], sem).wait()
@@ -216,8 +220,8 @@
     residual = (tokens[...].astype(F32) + total).astype(BF16).astype(F32)
     normed2 = rms_rows(residual, gain2[...]).astype(BF16)
     tk[z] = normed2
-    for p in zs:
-        send(TOK, tk.at[z], tk.at[z], (p * NC + yc, t))
+    for d in reversed(ring[1:]):
+        send(TOK, tk.at[z], tk.at[z], (at[d] * NC + yc, t), TOK2 if (NZ - d) % NZ in groups[1] else TOK)
 
     arrive(DENSE, d2, NZ - 1)
     for p in cores:
@@ -234,25 +238,28 @@
     for k in range(NT):
         own = jnp.where(t == k, residual[:, k * quarter : (k + 1) * quarter], own)
 
-    def stacked(ref, count):
-        return jnp.concatenate([ref[k].astype(F32) for k in range(count)], axis=0).astype(BF16)
+    def stacked(ref, offsets):
+        return jnp.concatenate([ref[at[d]].astype(F32) for d in offsets], axis=0).astype(BF16)
 
     arrive(ROUTE, rt, NZ - 1)
-    row, col = iota((R, R), 0), iota((R, R), 1)
-    pick = (col == z * 2 * NC + 2 * (row // (2 * NZ)) + lax.rem(row, 2)).astype(BF16)
-    same = lax.rem(iota((R, NZ * S), 0) // 2, NZ) == iota((R, NZ * S), 1) // S
-    take = jnp.where(same, dot_nt(pick, stacked(rt, NZ)), 0.0).astype(BF16)
-
-    arrive(TOK, tk, NZ - 1)
-    toks = stacked(tk, NZ)
-    bs_[...] = dot(take, toks).astype(BF16).reshape(bs_.shape)
-    for p in cores:
-        send(SLOT, bs_.at[p], br.at[yc], (z * NC + p, t))
-    br[yc] = bs_[yc]
+    rows_g = NC * half * 2
+    row, col = iota((rows_g, R), 0), iota((rows_g, R), 1)
+    pick = (col == z * 2 * NC + 2 * (row // (2 * half)) + lax.rem(row, 2)).astype(BF16)
+    same = lax.rem(iota((rows_g, half * S), 0) // 2, half) == iota((rows_g, half * S), 1) // S
+    takes = [jnp.where(same, dot_nt(pick, stacked(rt, group)), 0.0).astype(BF16) for group in groups]
+
+    toks = []
+    for k, group in enumerate(groups):
+        arrive((TOK, TOK2)[k], tk, len(group) - (k == 0))
+        toks.append(stacked(tk, group))
+        bs_[k] = dot(takes[k], toks[k]).astype(BF16).reshape(bs_.shape[1:])
+        for p in cores:
+            send((SLOT, SLOT2)[k], bs_.at[k, p], br.at[k, yc], (z * NC + p, t))
+        br[k, yc] = bs_[k, yc]
 
     arrive(DENSE2, d3, NZ * (NC - 1) // NC)
     dense_w = d3[...].reshape(D, 128)
-    pre = dot(toks, dense_w)
+    pre = dot(jnp.concatenate(toks, axis=0), dense_w)
     act = silu(pltpu.roll(pre, 2 * hs, 1)) * pltpu.roll(pre, hs, 1)
     lane = iota(act.shape, 1)
     act = jnp.where(jnp.logical_and(lane >= 2 * hs, lane < 3 * hs), act, 0.0).astype(BF16)
@@ -260,26 +267,37 @@
     for k in range(NZ):
         for j in range(NT):
             fs_[k * NT + j] = out[k * S : (k + 1) * S, j * quarter : (j + 1) * quarter].astype(BF16)
-    for d in range(1, NZ * NT):
-        p, q = lax.rem(z + d // NT, NZ), lax.rem(t + d % NT, NT)
-        send(DOUT, fs_.at[p * NT + q], fr.at[z * NT + t], (p * NC + yc, q))
-    fr[z * NT + t] = fs_[z * NT + t]
+    for k in reversed(range(NZ)):
+        for d in range(NT):
+            if ring[k] or d:
+                q = lax.rem(t + d, NT)
+                send(DOUT, fs_.at[k * NT + q], fr.at[z * NT + t], (at[ring[k]] * NC + yc, q))
+    fr[z * NT + t] = fs_[t]
 
     loads["g"].wait()
     loads["u"].wait()
-    arrive(SLOT, br, NC - 1)
-    arrived = br[...].reshape(R, D)
-    aa[t] = (silu(dot(arrived, vg[...])) * dot(arrived, vu[...])).astype(BF16)
-    for p in ts:
-        send(HID, aa.at[t], aa.at[t], (e, p))
+    for k in range(2):
+        arrive((SLOT, SLOT2)[k], br.at[k], NC - 1)
+        arrived = br[k].reshape(rows_g, D)
+        aa[k, t] = (silu(dot(arrived, vg[...])) * dot(arrived, vu[...])).astype(BF16)
+        for p in ts:
+            send((HID, HID2)[k], aa.at[k, t], aa.at[k, t], (e, p))
 
     arrive(DOWN, dq, NT - 1)
     down = jnp.concatenate([dq[k] for k in range(NT)], axis=0)
-    arrive(HID, aa, NT - 1)
-    hidden = jnp.concatenate([aa[k] for k in range(NT)], axis=1)
-    gs_[...] = dot(hidden, down).astype(BF16).reshape(gs_.shape)
-    each_ep(NE, lambda p: send(RET, gs_.at[lax.rem(p, NC) * NZ + p // NC], gr.at[e], (p, t)))
-    gr[e] = gs_[yc * NZ + z]
+    for k, group in enumerate(groups):
+        arrive((HID, HID2)[k], aa.at[k], NT - 1)
+        hidden = jnp.concatenate([aa[k, j] for j in range(NT)], axis=1)
+        gs_[k] = dot(hidden, down).astype(BF16).reshape(gs_.shape[1:])
+        for i in reversed(range(half)):
+
+            def back(j, c):
+                p = lax.rem(yc + j, NC)
+                send(RET, gs_.at[k, p * half + i], gr.at[e], (at[group[i]] * NC + p, t))
+                return c
+
+            lax.fori_loop(0 if group[i] else 1, NC, back, 0)
+    gr[e] = gs_[0, yc * half]
 
     arrive(DOUT, fr, NZ * NT - 1)
     dense = jnp.zeros((S, quarter), F32)
@@ -289,7 +307,7 @@
     arrive(RET, gr, NE - 1)
     mixed[...] = (base + dot(give.astype(BF16), gr[...].reshape(R, quarter))).astype(BF16)
 
-    for i, ref, count in ((PART, pt, NT - 1), (ROUTE, rt, NZ - 1), (DENSE, d1, NZ - 1), (DENSE2, d3, NZ * (NC - 1) // NC), (DOWN, dq, NT - 1), (TOK, tk, NZ - 1), (SLOT, bs_, NC - 1), (HID, aa, NT - 1), (RET, gs_, NE - 1)):
+    for i, ref, count in ((PART, pt, NT - 1), (ROUTE, rt, NZ - 1), (DENSE, d1, NZ - 1), (DENSE2, d3, NZ * (NC - 1) // NC), (DOWN, dq, NT - 1), (TOK, tk, NZ - 1), (SLOT, bs_.at[0], NC - 1), (SLOT2, bs_.at[1], NC - 1), (HID, aa.at[0], NT - 1), (HID2, aa.at[1], NT - 1), (RET, gr, NE - 1)):
         wait(ssem.at[i], ref, count)
     wait(ssem.at[DOUT], fr, NZ * NT - 1)
 
@@ -337,10 +355,10 @@
             half(D, inner), half(D, inner), half(D, cols), half(D, cols), pltpu.VMEM(ssm_state.shape, F32),
             half(inner, D), half(D, hidden), half(D, hidden), half(hidden, D),
             half(NT, S, D), half(NZ, rows, 128), half(NZ, rows, 128), half(NZ, NC, rows, 128), half(NT, hidden, quarter),
-            half(NZ, S, D), half(NZ, S, R), half(NC, 2 * NZ, D), half(NC, 2 * NZ, D), half(NT, R, hidden),
+            half(NZ, S, D), half(NZ, S, R), half(2, NC, NZ, D), half(2, NC, NZ, D), half(2, NT, R // 2, hidden),
             half(NZ * NT, S, quarter), half(NZ * NT, S, quarter),
-            half(NE, 2, quarter), half(NE, 2, quarter),
-            dma((8,)), dma((S,)), dma((20,)), dma((10,)), dma((10,)),
+            half(2, NE // 2, 2, quarter), half(NE, 2, quarter),
+            dma((8,)), dma((S,)), dma((20,)), dma((13,)), dma((13,)),
         ],
         compiler_params=pltpu.CompilerParams(collective_id=0, has_side_effects=True, vmem_limit_bytes=VMEM_STEP),
     )(

time: 41 us -> 39.9 us (0.973)
  Pallas kernels: 40.3 us -> 39.2 us
    pallas_call x1, Pallas kernels: 38.9 us -> 37.8 us  [body(): pl.pallas_call(functools.partial(step_kernel, NE, NC, NT, cols // sd), na...]
where the time goes in v4:
time: 39.9 us
  Pallas kernels  39.2 us (98%)
  between operations  0.65 us (2%)
    pallas_call x1, Pallas kernels, body(): pl.pallas_call(functools.partial(step_kernel, NE, NC, NT, cols // sd), na...  37.8 us
    pallas_call x1, Pallas kernels, body(): pl.pallas_call(functools.partial(store_kernel, len(made)), name='store',...  1.38 us

profile of v4, /device:TPU:1, one launch (start us, length us, event | category | flops | bytes accessed | tf_op | source)
XLA Modules:
  0.0 39.9 jit_solution(5788044228546118332)
XLA Ops:
  0.6 37.8 %step.1 = (bf16[8,256]{1,0:T(8,128)(2,1)S(1)}, f32[8,8,64,128]{3,2,1,0:T(8,128)S(1)}, bf16[3,8,512]{2,1,0:T(8,128)(2,1)S(1)}, bf16[3,8,256]{2,1,0:T(8,128)(2,1)S(1)}, bf16[3,8,256]{2,1,0:T(8,128)(2,1)S(1)}) custom-call(bf16[8,1024]{1,0:T(8,128)(2,1)} %refs_0_.1, bf16[3,8,512]{2,1,0:T(8,128)(2,1)} %bitcast.16, bf16[3,8,256]{2,1,0:T(8,128)(2,1)} %bitcast.17, ...), custom_call_target="tpu_custom_call" | custom-call | tf_op jit(solution)/shard_map/step/pallas_call | solution.py:345
  38.5 1.4 %store.1 = (bf16[8,256]{1,0:T(8,128)(2,1)}, f32[8,8,64,128]{3,2,1,0:T(8,128)}, bf16[3,8,512]{2,1,0:T(8,128)(2,1)}, bf16[3,8,256]{2,1,0:T(8,128)(2,1)}, bf16[3,8,256]{2,1,0:T(8,128)(2,1)}) custom-call(bf16[8,256]{1,0:T(8,128)(2,1)S(1)} %get-tuple-element.15.refs_0_, f32[8,8,64,128]{3,2,1,0:T(8,128)S(1)} %get-tuple-element.16.refs_1_, ...), custom_call_target="tpu_custom_call" | custom-call | tf_op jit(solution)/shard_map/store/pallas_call | solution.py:368

commit v5 on v4

--- a/solution.py
+++ b/solution.py
@@ -56,6 +56,18 @@
     z = e // NC
     yc = lax.rem(e, NC)
 
+    ts = [lax.rem(t + d, NT) for d in range(1, NT)]
+    ring = sorted(range(NZ), key=lambda d: (min(d, NZ - d), d))
+    half = NZ // 2
+    groups = (ring[:half], ring[half:])
+    at = [lax.rem(z + d, NZ) for d in range(NZ)]
+    zs = [at[d] for d in reversed(ring) if d]
+    around = [lax.rem(yc + d, NC) for d in range(NC)]
+    cores = around[1:]
+    barrier = pltpu.get_barrier_semaphore()
+    for dev in [(p * NC + yc, t) for p in zs] + [(z * NC + p, t) for p in cores] + [(e, p) for p in ts]:
+        pl.semaphore_signal(barrier, inc=1, device_id=dev, device_id_type=MESH)
+
     loads = {}
     for i, (name, src, dst) in enumerate((
         ("x", w_x, vx), ("b", w_b, vb), ("c", w_c, vc), ("z", w_z, vz), ("o", w_out, vo), ("d", w_d.at[0], vd), ("g", w_g.at[0], vg), ("u", w_u.at[0], vu)
@@ -64,42 +76,16 @@
     tiny = [pltpu.make_async_copy(src, dst, tsem.at[i]) for i, (src, dst) in enumerate(zip(given, small))]
     for c in tiny[:12]:
         c.start()
-    for name in "xbc":
+    for name in "xbcz":
         loads[name].start()
     ins = [pltpu.make_async_copy(state.at[s], st.at[s], isem.at[s]) for s in range(S)]
     for c in ins:
         c.start()
-    for name in "zo":
-        loads[name].start()
+    loads["o"].start()
     for c in tiny[12:]:
         c.start()
     for name in "dgu":
         loads[name].start()
-
-    barrier = pltpu.get_barrier_semaphore()
-
-    def greet(dev):
-        pl.semaphore_signal(barrier, inc=1, device_id=dev, device_id_type=MESH)
-
-    def each_ep(count, start):
-        def one(k, c):
-            half = (k + 1) // 2
-            start(lax.rem(e + count // 2 + (1 - 2 * lax.rem(k, 2)) * half, count))
-            return c
-
-        lax.fori_loop(0, count - 1, one, 0)
-
-    each_ep(NE, lambda p: greet((p, t)))
-    ts = [lax.rem(t + d, NT) for d in range(1, NT)]
-    ring = sorted(range(NZ), key=lambda d: (min(d, NZ - d), d))
-    half = NZ // 2
-    groups = (ring[:half], ring[half:])
-    at = [lax.rem(z + d, NZ) for d in range(NZ)]
-    zs = [at[d] for d in reversed(ring) if d]
-    cores = [lax.rem(yc + d, NC) for d in range(1, NC)]
-    for d in range(NZ):
-        for p in ts:
-            greet((lax.rem(z + d, NZ) * NC + yc, p))
 
     PART, ROUTE, DENSE, DENSE2, DOWN, TOK, SLOT, DOUT, HID, RET, TOK2, SLOT2, HID2 = range(13)
 
@@ -137,24 +123,25 @@
             out[j] = prev[j + 1] if j + 1 < depth else fresh
         return silu(total)
 
-    loads["x"].wait()
+    for name in "xbc":
+        loads[name].wait()
     xs = conv(conv_x, dot(normed, vx[...]), taps_x, cx_out)
-    loads["b"].wait()
     bs = conv(conv_b, dot(normed, vb[...]), taps_b, cb_out)
-    loads["c"].wait()
     cs = conv(conv_c, dot(normed, vc[...]), taps_c, cc_out)
     inflow = step * xs
+    loads["z"].wait()
+    zz = dot(normed, vz[...]).astype(BF16).astype(F32)
     rows = per * hd
     lane = iota((rows, S), 1)
     reads = [jnp.zeros((rows, S), F32) for _ in range(n_groups)]
     for s in range(S):
-        ins[s].wait()
+        if s % 4 == 0:
+            for c in ins[s : s + 4]:
+                c.wait()
         for g in range(n_groups):
             old = st[s, g * per : (g + 1) * per].reshape(rows, sd)
             got = jnp.sum(old * cs[s : s + 1, g * sd : (g + 1) * sd], axis=1, keepdims=True)
             reads[g] = jnp.where(lane == s, got, reads[g])
-    loads["z"].wait()
-    zz = dot(normed, vz[...]).astype(BF16).astype(F32)
     both = [jnp.sum(bs[:, g * sd : (g + 1) * sd] * cs[:, g * sd : (g + 1) * sd], axis=1, keepdims=True) for g in range(n_groups)]
     for c in tiny[12:]:
         c.wait()
@@ -168,7 +155,7 @@
     loads["o"].wait()
     pt[t] = dot(mixed_heads, vo[...]).astype(BF16)
 
-    pl.semaphore_wait(barrier, (NE - 1) + NZ * (NT - 1))
+    pl.semaphore_wait(barrier, (NZ - 1) + (NC - 1) + (NT - 1))
     for p in ts:
         send(PART, pt.at[t], pt.at[t], (e, p))
 
@@ -291,12 +278,8 @@
         gs_[k] = dot(hidden, down).astype(BF16).reshape(gs_.shape[1:])
         for i in reversed(range(half)):
 
-            def back(j, c):
-                p = lax.rem(yc + j, NC)
-                send(RET, gs_.at[k, p * half + i], gr.at[e], (at[group[i]] * NC + p, t))
-                return c
-
-            lax.fori_loop(0 if group[i] else 1, NC, back, 0)
+            for j in range(0 if group[i] else 1, NC):
+                send(RET, gs_.at[k, around[j] * half + i], gr.at[e], (at[group[i]] * NC + around[j], t))
     gr[e] = gs_[0, yc * half]
 
     arrive(DOUT, fr, NZ * NT - 1)

time: 39.9 us -> 37.4 us (0.937)
  Pallas kernels: 39.2 us -> 36.5 us
    pallas_call x1, Pallas kernels: 37.8 us -> 35.2 us  [body(): pl.pallas_call(functools.partial(step_kernel, NE, NC, NT, cols // sd), na...]
where the time goes in v5:
time: 37.4 us; the launch traced here: 37.2 us
  Pallas kernels  36.5 us (98%)
  between operations  0.65 us (2%)
    pallas_call x1, Pallas kernels, body(): pl.pallas_call(functools.partial(step_kernel, NE, NC, NT, cols // sd), na...  35.2 us
    pallas_call x1, Pallas kernels, body(): pl.pallas_call(functools.partial(store_kernel, len(made)), name='store',...  1.38 us

profile of v5, /device:TPU:1, one launch (start us, length us, event | category | flops | bytes accessed | tf_op | source)
XLA Modules:
  0.0 37.2 jit_solution(5620789154666266602)
XLA Ops:
  0.6 35.2 %step.1 = (bf16[8,256]{1,0:T(8,128)(2,1)S(1)}, f32[8,8,64,128]{3,2,1,0:T(8,128)S(1)}, bf16[3,8,512]{2,1,0:T(8,128)(2,1)S(1)}, bf16[3,8,256]{2,1,0:T(8,128)(2,1)S(1)}, bf16[3,8,256]{2,1,0:T(8,128)(2,1)S(1)}) custom-call(bf16[8,1024]{1,0:T(8,128)(2,1)} %refs_0_.1, bf16[3,8,512]{2,1,0:T(8,128)(2,1)} %bitcast.16, bf16[3,8,256]{2,1,0:T(8,128)(2,1)} %bitcast.17, ...), custom_call_target="tpu_custom_call" | custom-call | tf_op jit(solution)/shard_map/step/pallas_call | solution.py:328
  35.8 1.4 %store.1 = (bf16[8,256]{1,0:T(8,128)(2,1)}, f32[8,8,64,128]{3,2,1,0:T(8,128)}, bf16[3,8,512]{2,1,0:T(8,128)(2,1)}, bf16[3,8,256]{2,1,0:T(8,128)(2,1)}, bf16[3,8,256]{2,1,0:T(8,128)(2,1)}) custom-call(bf16[8,256]{1,0:T(8,128)(2,1)S(1)} %get-tuple-element.15.refs_0_, f32[8,8,64,128]{3,2,1,0:T(8,128)S(1)} %get-tuple-element.16.refs_1_, ...), custom_call_target="tpu_custom_call" | custom-call | tf_op jit(solution)/shard_map/store/pallas_call | solution.py:351

commit v6 on v5

--- a/solution.py
+++ b/solution.py
@@ -129,15 +129,16 @@
     bs = conv(conv_b, dot(normed, vb[...]), taps_b, cb_out)
     cs = conv(conv_c, dot(normed, vc[...]), taps_c, cc_out)
     inflow = step * xs
+    rows = per * hd
     loads["z"].wait()
-    zz = dot(normed, vz[...]).astype(BF16).astype(F32)
-    rows = per * hd
     lane = iota((rows, S), 1)
     reads = [jnp.zeros((rows, S), F32) for _ in range(n_groups)]
     for s in range(S):
         if s % 4 == 0:
             for c in ins[s : s + 4]:
                 c.wait()
+        if s == 0:
+            zz = dot(normed, vz[...]).astype(BF16).astype(F32)
         for g in range(n_groups):
             old = st[s, g * per : (g + 1) * per].reshape(rows, sd)
             got = jnp.sum(old * cs[s : s + 1, g * sd : (g + 1) * sd], axis=1, keepdims=True)
@@ -187,9 +188,6 @@
         send(DENSE, d1.at[p], d2.at[z], (p * NC + yc, t))
     d2[z] = d1[z]
     loads["d"].wait()
-    for p in ts:
-        send(DOWN, vd.at[:, pl.ds(pl.multiple_of(p * quarter, quarter), quarter)], dq.at[t], (e, p))
-    dq[t] = vd[:, pl.ds(pl.multiple_of(t * quarter, quarter), quarter)]
 
     in_col = inflow.T
     decay_col = decay.T
@@ -209,6 +207,10 @@
     tk[z] = normed2
     for d in reversed(ring[1:]):
         send(TOK, tk.at[z], tk.at[z], (at[d] * NC + yc, t), TOK2 if (NZ - d) % NZ in groups[1] else TOK)
+
+    for p in ts:
+        send(DOWN, vd.at[:, pl.ds(pl.multiple_of(p * quarter, quarter), quarter)], dq.at[t], (e, p))
+    dq[t] = vd[:, pl.ds(pl.multiple_of(t * quarter, quarter), quarter)]
 
     arrive(DENSE, d2, NZ - 1)
     for p in cores:

time: 37.4 us -> 37.3 us (level)
  no operation moved by 1% of the time
where the time goes in v6:
time: 37.3 us; the launch traced here: 37.1 us
  Pallas kernels  36.4 us (98%)
  between operations  0.65 us (2%)
    pallas_call x1, Pallas kernels, body(): pl.pallas_call(functools.partial(step_kernel, NE, NC, NT, cols // sd), na...  35.1 us
    pallas_call x1, Pallas kernels, body(): pl.pallas_call(functools.partial(store_kernel, len(made)), name='store',...  1.38 us

profile of v6, /device:TPU:1, one launch (start us, length us, event | category | flops | bytes accessed | tf_op | source)
XLA Modules:
  0.0 37.1 jit_solution(13149087922824538927)
XLA Ops:
  0.6 35.1 %step.1 = (bf16[8,256]{1,0:T(8,128)(2,1)S(1)}, f32[8,8,64,128]{3,2,1,0:T(8,128)S(1)}, bf16[3,8,512]{2,1,0:T(8,128)(2,1)S(1)}, bf16[3,8,256]{2,1,0:T(8,128)(2,1)S(1)}, bf16[3,8,256]{2,1,0:T(8,128)(2,1)S(1)}) custom-call(bf16[8,1024]{1,0:T(8,128)(2,1)} %refs_0_.1, bf16[3,8,512]{2,1,0:T(8,128)(2,1)} %bitcast.16, bf16[3,8,256]{2,1,0:T(8,128)(2,1)} %bitcast.17, ...), custom_call_target="tpu_custom_call" | custom-call | tf_op jit(solution)/shard_map/step/pallas_call | solution.py:330
  35.7 1.4 %store.1 = (bf16[8,256]{1,0:T(8,128)(2,1)}, f32[8,8,64,128]{3,2,1,0:T(8,128)}, bf16[3,8,512]{2,1,0:T(8,128)(2,1)}, bf16[3,8,256]{2,1,0:T(8,128)(2,1)}, bf16[3,8,256]{2,1,0:T(8,128)(2,1)}) custom-call(bf16[8,256]{1,0:T(8,128)(2,1)S(1)} %get-tuple-element.15.refs_0_, f32[8,8,64,128]{3,2,1,0:T(8,128)S(1)} %get-tuple-element.16.refs_1_, ...), custom_call_target="tpu_custom_call" | custom-call | tf_op jit(solution)/shard_map/store/pallas_call | solution.py:353

commit v7 on v6

--- a/solution.py
+++ b/solution.py
@@ -43,7 +43,7 @@
     small, refs = refs[14:34], refs[34:]
     tokens, conv_x, conv_b, conv_c, w_dt, dt_bias, a_log, d_skip, taps_x, taps_b, taps_c, gain = small[:12]
     ggain, gain2, ids, wts, dgate, dup, ddown, bgate = small[12:]
-    vx, vz, vb, vc, st, vo, vg, vu, vd, pt, d1, d2, d3, dq, tk, rt, bs_, br, aa, fs_, fr, gs_, gr, lsem, isem, tsem, ssem, rsem = refs
+    vx, vz, vb, vc, st, vo, vg, vu, vd, pt, d1, d2, d3, dq, tk, rt, bs_, br, aa, fs_, fx, fz, fr, gs_, gr, lsem, isem, tsem, ssem, rsem = refs
     NZ = NE // NC
     S, D = tokens.shape
     heads, hd, sd = st.shape[1:]
@@ -76,18 +76,19 @@
     tiny = [pltpu.make_async_copy(src, dst, tsem.at[i]) for i, (src, dst) in enumerate(zip(given, small))]
     for c in tiny[:12]:
         c.start()
-    for name in "xbcz":
+    for name in "xbc":
         loads[name].start()
+    for c in tiny[12:]:
+        c.start()
+    loads["z"].start()
     ins = [pltpu.make_async_copy(state.at[s], st.at[s], isem.at[s]) for s in range(S)]
     for c in ins:
         c.start()
     loads["o"].start()
-    for c in tiny[12:]:
-        c.start()
     for name in "dgu":
         loads[name].start()
 
-    PART, ROUTE, DENSE, DENSE2, DOWN, TOK, SLOT, DOUT, HID, RET, TOK2, SLOT2, HID2 = range(13)
+    PART, ROUTE, DENSE, DENSE2, DOWN, TOK, SLOT, DOUT, HID, RET, TOK2, SLOT2, HID2, DZ = range(14)
 
     def send(i, src, dst, dev, there=None):
         pltpu.make_async_remote_copy(src_ref=src, dst_ref=dst, send_sem=ssem.at[i], recv_sem=rsem.at[i if there is None else there], device_id=dev, device_id_type=MESH).start()
@@ -129,6 +130,37 @@
     bs = conv(conv_b, dot(normed, vb[...]), taps_b, cb_out)
     cs = conv(conv_c, dot(normed, vc[...]), taps_c, cc_out)
     inflow = step * xs
+    for c in tiny[12:]:
+        c.wait()
+    slot = iota((S, R), 1)
+    named = jnp.zeros((S, R), F32)
+    weight = jnp.zeros((S, R), F32)
+    for k in range(ids.shape[1]):
+        hit = ids[:, k : k + 1] == slot // 2
+        named = jnp.where(hit, 1.0, named)
+        weight = jnp.where(hit, wts[:, k : k + 1], weight)
+    before = (iota((S, S), 0) > iota((S, S), 1)).astype(F32)
+    rank = dot(before, named)
+    mine = jnp.logical_and(named > 0.5, jnp.abs(rank - lax.rem(slot, 2).astype(F32)) < 0.5)
+    rt[z] = jnp.where(mine, 1.0, 0.0).astype(BF16)
+    give = jnp.where(mine, weight, 0.0)
+    hs = dgate.shape[1] // NZ
+    lane = iota((dgate.shape[0], 128), 1)
+    three = [dgate[...].astype(F32), dup[...].astype(F32), ddown[...].astype(F32)]
+    for k in range(NZ):
+        page, off = k * hs // 128 * 128, k * hs % 128
+        block = jnp.zeros(lane.shape, F32)
+        for j, v in enumerate(three):
+            v = v[:, page : page + 128]
+            shift = (j * hs - off) % 128
+            block = jnp.where(jnp.logical_and(lane >= j * hs, lane < (j + 1) * hs), pltpu.roll(v, shift, 1) if shift else v, block)
+        d1[k] = block.astype(BF16)
+    pl.semaphore_wait(barrier, (NZ - 1) + (NC - 1) + (NT - 1))
+    for p in zs:
+        send(ROUTE, rt.at[z], rt.at[z], (p * NC + yc, t))
+        send(DENSE, d1.at[p], d2.at[z], (p * NC + yc, t))
+    d2[z] = d1[z]
+
     rows = per * hd
     loads["z"].wait()
     lane = iota((rows, S), 1)
@@ -144,8 +176,6 @@
             got = jnp.sum(old * cs[s : s + 1, g * sd : (g + 1) * sd], axis=1, keepdims=True)
             reads[g] = jnp.where(lane == s, got, reads[g])
     both = [jnp.sum(bs[:, g * sd : (g + 1) * sd] * cs[:, g * sd : (g + 1) * sd], axis=1, keepdims=True) for g in range(n_groups)]
-    for c in tiny[12:]:
-        c.wait()
     parts = []
     for g in range(n_groups):
         cut = slice(g * rows, (g + 1) * rows)
@@ -156,37 +186,9 @@
     loads["o"].wait()
     pt[t] = dot(mixed_heads, vo[...]).astype(BF16)
 
-    pl.semaphore_wait(barrier, (NZ - 1) + (NC - 1) + (NT - 1))
     for p in ts:
         send(PART, pt.at[t], pt.at[t], (e, p))
 
-    slot = iota((S, R), 1)
-    named = jnp.zeros((S, R), F32)
-    weight = jnp.zeros((S, R), F32)
-    for k in range(ids.shape[1]):
-        hit = ids[:, k : k + 1] == slot // 2
-        named = jnp.where(hit, 1.0, named)
-        weight = jnp.where(hit, wts[:, k : k + 1], weight)
-    before = (iota((S, S), 0) > iota((S, S), 1)).astype(F32)
-    rank = dot(before, named)
-    mine = jnp.logical_and(named > 0.5, jnp.abs(rank - lax.rem(slot, 2).astype(F32)) < 0.5)
-    rt[z] = jnp.where(mine, 1.0, 0.0).astype(BF16)
-    give = jnp.where(mine, weight, 0.0)
-    hs = dgate.shape[1] // NZ
-    lane = iota((dgate.shape[0], 128), 1)
-    three = [dgate[...].astype(F32), dup[...].astype(F32), ddown[...].astype(F32)]
-    for k in range(NZ):
-        page, off = k * hs // 128 * 128, k * hs % 128
-        block = jnp.zeros(lane.shape, F32)
-        for j, v in enumerate(three):
-            v = v[:, page : page + 128]
-            shift = (j * hs - off) % 128
-            block = jnp.where(jnp.logical_and(lane >= j * hs, lane < (j + 1) * hs), pltpu.roll(v, shift, 1) if shift else v, block)
-        d1[k] = block.astype(BF16)
-    for p in zs:
-        send(ROUTE, rt.at[z], rt.at[z], (p * NC + yc, t))
-        send(DENSE, d1.at[p], d2.at[z], (p * NC + yc, t))
-    d2[z] = d1[z]
     loads["d"].wait()
 
     in_col = inflow.T
@@ -197,6 +199,12 @@
             old = st[s, g * per : (g + 1) * per].reshape(rows, sd)
             new = decay_col[cut, s : s + 1] * old + in_col[cut, s : s + 1] * bs[s : s + 1, g * sd : (g + 1) * sd]
             state_out[s, g * per : (g + 1) * per] = new.reshape(per, hd, sd)
+
+    arrive(DENSE, d2, NZ - 1)
+    for p in cores:
+        send(DENSE2, d2, d3.at[:, yc], (z * NC + p, t))
+    for k in range(NZ):
+        d3[k, yc] = d2[k]
 
     arrive(PART, pt, NT - 1)
     total = pt[0].astype(F32)
@@ -212,12 +220,6 @@
         send(DOWN, vd.at[:, pl.ds(pl.multiple_of(p * quarter, quarter), quarter)], dq.at[t], (e, p))
     dq[t] = vd[:, pl.ds(pl.multiple_of(t * quarter, quarter), quarter)]
 
-    arrive(DENSE, d2, NZ - 1)
-    for p in cores:
-        send(DENSE2, d2, d3.at[:, yc], (z * NC + p, t))
-    for k in range(NZ):
-        d3[k, yc] = d2[k]
-
     lanes = bgate.shape[1]
     weighted = jnp.zeros((S, lanes), F32)
     for k in range(bgate.shape[0]):
@@ -255,13 +257,10 @@
     out = dot_nt(act, dense_w)
     for k in range(NZ):
         for j in range(NT):
-            fs_[k * NT + j] = out[k * S : (k + 1) * S, j * quarter : (j + 1) * quarter].astype(BF16)
-    for k in reversed(range(NZ)):
-        for d in range(NT):
-            if ring[k] or d:
-                q = lax.rem(t + d, NT)
-                send(DOUT, fs_.at[k * NT + q], fr.at[z * NT + t], (at[ring[k]] * NC + yc, q))
-    fr[z * NT + t] = fs_[t]
+            fs_[j, k] = out[k * S : (k + 1) * S, j * quarter : (j + 1) * quarter].astype(BF16)
+    for p in ts:
+        send(DOUT, fs_.at[p], fx.at[t], (e, p))
+    fx[t] = fs_[t]
 
     loads["g"].wait()
     loads["u"].wait()
@@ -272,6 +271,16 @@
         for p in ts:
             send((HID, HID2)[k], aa.at[k, t], aa.at[k, t], (e, p))
 
+    arrive(DOUT, fx, NT - 1)
+    for k in range(NZ):
+        v = fx[0, k].astype(F32)
+        for j in range(1, NT):
+            v = v + fx[j, k].astype(F32)
+        fz[k] = v.astype(BF16)
+    for k in reversed(range(1, NZ)):
+        send(DZ, fz.at[k], fr.at[z], (at[ring[k]] * NC + yc, t))
+    fr[z] = fz[0]
+
     arrive(DOWN, dq, NT - 1)
     down = jnp.concatenate([dq[k] for k in range(NT)], axis=0)
     for k, group in enumerate(groups):
@@ -284,9 +293,9 @@
                 send(RET, gs_.at[k, around[j] * half + i], gr.at[e], (at[group[i]] * NC + around[j], t))
     gr[e] = gs_[0, yc * half]
 
-    arrive(DOUT, fr, NZ * NT - 1)
+    arrive(DZ, fr, NZ - 1)
     dense = jnp.zeros((S, quarter), F32)
-    for k in range(NZ * NT):
+    for k in range(NZ):
         dense = dense + fr[k].astype(F32)
     base = own + branch * dense
     arrive(RET, gr, NE - 1)
@@ -294,7 +303,8 @@
 
     for i, ref, count in ((PART, pt, NT - 1), (ROUTE, rt, NZ - 1), (DENSE, d1, NZ - 1), (DENSE2, d3, NZ * (NC - 1) // NC), (DOWN, dq, NT - 1), (TOK, tk, NZ - 1), (SLOT, bs_.at[0], NC - 1), (SLOT2, bs_.at[1], NC - 1), (HID, aa.at[0], NT - 1), (HID2, aa.at[1], NT - 1), (RET, gr, NE - 1)):
         wait(ssem.at[i], ref, count)
-    wait(ssem.at[DOUT], fr, NZ * NT - 1)
+    wait(ssem.at[DOUT], fx, NT - 1)
+    wait(ssem.at[DZ], fr, NZ - 1)
 
 
 def store_kernel(count, *refs):
@@ -341,9 +351,9 @@
             half(inner, D), half(D, hidden), half(D, hidden), half(hidden, D),
             half(NT, S, D), half(NZ, rows, 128), half(NZ, rows, 128), half(NZ, NC, rows, 128), half(NT, hidden, quarter),
             half(NZ, S, D), half(NZ, S, R), half(2, NC, NZ, D), half(2, NC, NZ, D), half(2, NT, R // 2, hidden),
-            half(NZ * NT, S, quarter), half(NZ * NT, S, quarter),
+            half(NT, NZ, S, quarter), half(NT, NZ, S, quarter), half(NZ, S, quarter), half(NZ, S, quarter),
             half(2, NE // 2, 2, quarter), half(NE, 2, quarter),
-            dma((8,)), dma((S,)), dma((20,)), dma((13,)), dma((13,)),
+            dma((8,)), dma((S,)), dma((20,)), dma((14,)), dma((14,)),
         ],
         compiler_params=pltpu.CompilerParams(collective_id=0, has_side_effects=True, vmem_limit_bytes=VMEM_STEP),
     )(

time: 37.3 us -> 37.6 us (level)
  no operation moved by 1% of the time
where the time goes in v7:
time: 37.6 us; the launch traced here: 37.4 us
  Pallas kernels  36.7 us (98%)
  between operations  0.65 us (2%)
    pallas_call x1, Pallas kernels, body(): pl.pallas_call(functools.partial(step_kernel, NE, NC, NT, cols // sd), na...  35.4 us
    pallas_call x1, Pallas kernels, body(): pl.pallas_call(functools.partial(store_kernel, len(made)), name='store',...  1.38 us

profile of v7, /device:TPU:1, one launch (start us, length us, event | category | flops | bytes accessed | tf_op | source)
XLA Modules:
  0.0 37.4 jit_solution(14235981930071292863)
XLA Ops:
  0.6 35.4 %step.1 = (bf16[8,256]{1,0:T(8,128)(2,1)S(1)}, f32[8,8,64,128]{3,2,1,0:T(8,128)S(1)}, bf16[3,8,512]{2,1,0:T(8,128)(2,1)S(1)}, bf16[3,8,256]{2,1,0:T(8,128)(2,1)S(1)}, bf16[3,8,256]{2,1,0:T(8,128)(2,1)S(1)}) custom-call(bf16[8,1024]{1,0:T(8,128)(2,1)} %refs_0_.1, bf16[3,8,512]{2,1,0:T(8,128)(2,1)} %bitcast.16, bf16[3,8,256]{2,1,0:T(8,128)(2,1)} %bitcast.17, ...), custom_call_target="tpu_custom_call" | custom-call | tf_op jit(solution)/shard_map/step/pallas_call | solution.py:340
  36.0 1.4 %store.1 = (bf16[8,256]{1,0:T(8,128)(2,1)}, f32[8,8,64,128]{3,2,1,0:T(8,128)}, bf16[3,8,512]{2,1,0:T(8,128)(2,1)}, bf16[3,8,256]{2,1,0:T(8,128)(2,1)}, bf16[3,8,256]{2,1,0:T(8,128)(2,1)}) custom-call(bf16[8,256]{1,0:T(8,128)(2,1)S(1)} %get-tuple-element.15.refs_0_, f32[8,8,64,128]{3,2,1,0:T(8,128)S(1)} %get-tuple-element.16.refs_1_, ...), custom_call_target="tpu_custom_call" | custom-call | tf_op jit(solution)/shard_map/store/pallas_call | solution.py:363

commit v8 on v6

--- a/solution.py
+++ b/solution.py
@@ -43,7 +43,7 @@
     small, refs = refs[14:34], refs[34:]
     tokens, conv_x, conv_b, conv_c, w_dt, dt_bias, a_log, d_skip, taps_x, taps_b, taps_c, gain = small[:12]
     ggain, gain2, ids, wts, dgate, dup, ddown, bgate = small[12:]
-    vx, vz, vb, vc, st, vo, vg, vu, vd, pt, d1, d2, d3, dq, tk, rt, bs_, br, aa, fs_, fr, gs_, gr, lsem, isem, tsem, ssem, rsem = refs
+    vx, vz, vb, vc, st, vo, vg, vu, vd, pt, d1, d2, d3, dq, tk, rt, bs_, br, aa, fs_, fx, fz, fr, gs_, gr, lsem, isem, tsem, ssem, rsem = refs
     NZ = NE // NC
     S, D = tokens.shape
     heads, hd, sd = st.shape[1:]
@@ -87,7 +87,7 @@
     for name in "dgu":
         loads[name].start()
 
-    PART, ROUTE, DENSE, DENSE2, DOWN, TOK, SLOT, DOUT, HID, RET, TOK2, SLOT2, HID2 = range(13)
+    PART, ROUTE, DENSE, DENSE2, DOWN, TOK, SLOT, DOUT, HID, RET, TOK2, SLOT2, HID2, DZ = range(14)
 
     def send(i, src, dst, dev, there=None):
         pltpu.make_async_remote_copy(src_ref=src, dst_ref=dst, send_sem=ssem.at[i], recv_sem=rsem.at[i if there is None else there], device_id=dev, device_id_type=MESH).start()
@@ -255,13 +255,10 @@
     out = dot_nt(act, dense_w)
     for k in range(NZ):
         for j in range(NT):
-            fs_[k * NT + j] = out[k * S : (k + 1) * S, j * quarter : (j + 1) * quarter].astype(BF16)
-    for k in reversed(range(NZ)):
-        for d in range(NT):
-            if ring[k] or d:
-                q = lax.rem(t + d, NT)
-                send(DOUT, fs_.at[k * NT + q], fr.at[z * NT + t], (at[ring[k]] * NC + yc, q))
-    fr[z * NT + t] = fs_[t]
+            fs_[j, k] = out[k * S : (k + 1) * S, j * quarter : (j + 1) * quarter].astype(BF16)
+    for p in ts:
+        send(DOUT, fs_.at[p], fx.at[t], (e, p))
+    fx[t] = fs_[t]
 
     loads["g"].wait()
     loads["u"].wait()
@@ -272,6 +269,16 @@
         for p in ts:
             send((HID, HID2)[k], aa.at[k, t], aa.at[k, t], (e, p))
 
+    arrive(DOUT, fx, NT - 1)
+    for k in range(NZ):
+        v = fx[0, k].astype(F32)
+        for j in range(1, NT):
+            v = v + fx[j, k].astype(F32)
+        fz[k] = v.astype(BF16)
+    for k in reversed(range(1, NZ)):
+        send(DZ, fz.at[k], fr.at[z], (at[ring[k]] * NC + yc, t))
+    fr[z] = fz[0]
+
     arrive(DOWN, dq, NT - 1)
     down = jnp.concatenate([dq[k] for k in range(NT)], axis=0)
     for k, group in enumerate(groups):
@@ -284,9 +291,9 @@
                 send(RET, gs_.at[k, around[j] * half + i], gr.at[e], (at[group[i]] * NC + around[j], t))
     gr[e] = gs_[0, yc * half]
 
-    arrive(DOUT, fr, NZ * NT - 1)
+    arrive(DZ, fr, NZ - 1)
     dense = jnp.zeros((S, quarter), F32)
-    for k in range(NZ * NT):
+    for k in range(NZ):
         dense = dense + fr[k].astype(F32)
     base = own + branch * dense
     arrive(RET, gr, NE - 1)
@@ -294,7 +301,8 @@
 
     for i, ref, count in ((PART, pt, NT - 1), (ROUTE, rt, NZ - 1), (DENSE, d1, NZ - 1), (DENSE2, d3, NZ * (NC - 1) // NC), (DOWN, dq, NT - 1), (TOK, tk, NZ - 1), (SLOT, bs_.at[0], NC - 1), (SLOT2, bs_.at[1], NC - 1), (HID, aa.at[0], NT - 1), (HID2, aa.at[1], NT - 1), (RET, gr, NE - 1)):
         wait(ssem.at[i], ref, count)
-    wait(ssem.at[DOUT], fr, NZ * NT - 1)
+    wait(ssem.at[DOUT], fx, NT - 1)
+    wait(ssem.at[DZ], fr, NZ - 1)
 
 
 def store_kernel(count, *refs):
@@ -341,9 +349,9 @@
             half(inner, D), half(D, hidden), half(D, hidden), half(hidden, D),
             half(NT, S, D), half(NZ, rows, 128), half(NZ, rows, 128), half(NZ, NC, rows, 128), half(NT, hidden, quarter),
             half(NZ, S, D), half(NZ, S, R), half(2, NC, NZ, D), half(2, NC, NZ, D), half(2, NT, R // 2, hidden),
-            half(NZ * NT, S, quarter), half(NZ * NT, S, quarter),
+            half(NT, NZ, S, quarter), half(NT, NZ, S, quarter), half(NZ, S, quarter), half(NZ, S, quarter),
             half(2, NE // 2, 2, quarter), half(NE, 2, quarter),
-            dma((8,)), dma((S,)), dma((20,)), dma((13,)), dma((13,)),
+            dma((8,)), dma((S,)), dma((20,)), dma((14,)), dma((14,)),
         ],
         compiler_params=pltpu.CompilerParams(collective_id=0, has_side_effects=True, vmem_limit_bytes=VMEM_STEP),
     )(

time: 37.3 us -> 36.5 us (0.979)
  Pallas kernels: 36.4 us -> 35.7 us
    pallas_call x1, Pallas kernels: 35.1 us -> 34.4 us  [body(): pl.pallas_call(functools.partial(step_kernel, NE, NC, NT, cols // sd), na...]
where the time goes in v8:
time: 36.5 us; the launch traced here: 36.4 us
  Pallas kernels  35.7 us (98%)
  between operations  0.65 us (2%)
    pallas_call x1, Pallas kernels, body(): pl.pallas_call(functools.partial(step_kernel, NE, NC, NT, cols // sd), na...  34.4 us
    pallas_call x1, Pallas kernels, body(): pl.pallas_call(functools.partial(store_kernel, len(made)), name='store',...  1.38 us

profile of v8, /device:TPU:1, one launch (start us, length us, event | category | flops | bytes accessed | tf_op | source)
XLA Modules:
  0.0 36.4 jit_solution(4463981890976061146)
XLA Ops:
  0.6 34.4 %step.1 = (bf16[8,256]{1,0:T(8,128)(2,1)S(1)}, f32[8,8,64,128]{3,2,1,0:T(8,128)S(1)}, bf16[3,8,512]{2,1,0:T(8,128)(2,1)S(1)}, bf16[3,8,256]{2,1,0:T(8,128)(2,1)S(1)}, bf16[3,8,256]{2,1,0:T(8,128)(2,1)S(1)}) custom-call(bf16[8,1024]{1,0:T(8,128)(2,1)} %refs_0_.1, bf16[3,8,512]{2,1,0:T(8,128)(2,1)} %bitcast.16, bf16[3,8,256]{2,1,0:T(8,128)(2,1)} %bitcast.17, ...), custom_call_target="tpu_custom_call" | custom-call | tf_op jit(solution)/shard_map/step/pallas_call | solution.py:338
  35.0 1.4 %store.1 = (bf16[8,256]{1,0:T(8,128)(2,1)}, f32[8,8,64,128]{3,2,1,0:T(8,128)}, bf16[3,8,512]{2,1,0:T(8,128)(2,1)}, bf16[3,8,256]{2,1,0:T(8,128)(2,1)}, bf16[3,8,256]{2,1,0:T(8,128)(2,1)}) custom-call(bf16[8,256]{1,0:T(8,128)(2,1)S(1)} %get-tuple-element.15.refs_0_, f32[8,8,64,128]{3,2,1,0:T(8,128)S(1)} %get-tuple-element.16.refs_1_, ...), custom_call_target="tpu_custom_call" | custom-call | tf_op jit(solution)/shard_map/store/pallas_call | solution.py:361
